TPU v7x, 256 devices: a whole 4x4x8 slice. The times are simulated.
256 devices in a mesh: ep: 64 (over z, y, core), tp: 4 (over x).
Axes of the slice: x: 4, y: 4, z: 8, core: 2. Of those that a mesh axis runs over, the one named last changes fastest.
Arguments:
- mix_input: bfloat16 [65536, 2048], P(('ep', 'tp')), may hold values from -6 to 6
- mix_gain: float32 [2048], replicated, may hold values from 0.1 to 1.9
- pool_weight: bfloat16 [4, 512, 512], replicated, may hold values from -0.25 to 0.25
- pool_scale: float32 [2048], replicated, may hold values from 0.1 to 1.9
- moe_input: bfloat16 [32768, 2048], P(('ep', 'tp')), may hold values from -6 to 6
- moe_gain: float32 [2048], replicated, may hold values from 0.1 to 1.9
- expert_ids: int32 [32768, 4], P('ep'), may hold values from 0 to 127, all different within a row; in each aligned block of 128 rows (0 to 127, 128 to 255, ...) at most 6 rows name the same one
- route_score: float32 [32768, 4], P(('ep', 'tp')), may hold values from 0.05 to 1
- expert_gate: bfloat16 [128, 2048, 1024], P('ep', None, 'tp'), may hold values from -0.125 to 0.125
- expert_up: bfloat16 [128, 2048, 1024], P('ep', None, 'tp'), may hold values from -0.125 to 0.125
- expert_down: bfloat16 [128, 1024, 2048], P('ep', 'tp'), may hold values from -0.1875 to 0.1875
- shared_gate: bfloat16 [2048, 512], P(None, 'tp'), may hold values from -0.125 to 0.125
- shared_up: bfloat16 [2048, 512], P(None, 'tp'), may hold values from -0.125 to 0.125
- shared_down: bfloat16 [512, 2048], P('tp'), may hold values from -0.25 to 0.25
Outputs:
- mix_output: bfloat16 [65536, 2048], P(('ep', 'tp'))
- moe_output: bfloat16 [32768, 2048], P(('ep', 'tp'))
Inputs may be any that keep to these rules, and one draw needn't show every extreme that they name: `expert_ids`: each row names 4 different experts. Within each aligned block of 128 rows (the tokens of one device) no expert is named by more than 6 rows, a bound that some block reaches.
All inputs are finite; a program needn't handle non-finite values.
Results may differ from a plain program's by a relative error of at most 0.012.
Values may be sent and summed in bfloat16 or wider, within the bound.
No kernel may reach another device: no remote copies, remote signals or barrier semaphores. Data moves between devices by JAX's collectives and lax.ppermute only.
A program may use at most 192 MiB of HBM per device.

v0:
```python
import jax
import jax.numpy as jnp
from jax import lax
from jax.sharding import PartitionSpec as P

WINDOWS = (2, 4, 8, 16)
RMS_EPS = 1e-06
ROUTED_SCALE = 2.5


def passed_along(value, axis, by):
    length = lax.axis_size(axis)
    pairs = [(i, i + by) for i in range(length) if 0 <= i + by < length]
    return lax.ppermute(value, axis, pairs)


def in_one_piece(arrays, axis, dim, along):
    ends, at = ([], 0)
    for a in arrays[:-1]:
        at += a.shape[along]
        ends.append(at)
    both = jnp.concatenate(arrays, axis=along)
    return tuple(jnp.split(lax.all_gather(both, axis, axis=dim, tiled=True), ends, axis=along))


def rms_norm(values, gain_row):
    upcast = values.astype(jnp.float32)
    scaled = upcast * lax.rsqrt(jnp.mean(upcast * upcast, axis=-1, keepdims=True) + RMS_EPS)
    return (scaled * gain_row).astype(jnp.bfloat16)


def rounded(values):
    return lax.optimization_barrier(values.astype(jnp.bfloat16)).astype(jnp.float32)


def window_means(normed, before, offset):
    row_count = normed.shape[0]
    lead_rows = before.shape[0]
    group_size = normed.shape[1] // len(WINDOWS)
    joined = jnp.concatenate([before, normed], axis=0).astype(jnp.float32)
    positions = offset + jnp.arange(row_count, dtype=jnp.int32)
    window_avg = []
    for group_idx, span in enumerate(WINDOWS):
        channels = joined[:, group_idx * group_size : (group_idx + 1) * group_size]
        first_row = lead_rows - span + 1
        running = channels[first_row : first_row + row_count]
        for shift_idx in range(1, span):
            running = running + channels[first_row + shift_idx : first_row + shift_idx + row_count]
        counts = jnp.minimum(positions + 1, span).astype(jnp.float32)
        window_avg.append(running / counts[:, None])
    return jnp.stack(window_avg, axis=1)


def fill_slots(normed, picks, expert_count, capacity):
    tok_count, top_count = picks.shape
    pair_count = tok_count * top_count
    flat_ids = picks.reshape(pair_count)
    matches = flat_ids[:, None] == jnp.arange(expert_count, dtype=jnp.int32)[None, :]
    pair_line = jnp.arange(pair_count, dtype=jnp.int32)
    lower_mask = (pair_line[:, None] > pair_line[None, :]).astype(jnp.bfloat16)
    seen_before = jnp.dot(
        lower_mask, matches.astype(jnp.bfloat16), preferred_element_type=jnp.float32
    )
    rank = jnp.sum(seen_before * matches.astype(jnp.float32), axis=1).astype(jnp.int32)
    slots = flat_ids * capacity + rank
    owner = pair_line // top_count
    slot_token = jnp.full((expert_count * capacity,), tok_count, jnp.int32).at[slots].set(owner)
    padded = jnp.concatenate([normed, jnp.zeros((1, normed.shape[1]), normed.dtype)], axis=0)
    return (padded[slot_token], slots.reshape(tok_count, top_count))


def blockwise_down(hidden, down_rows, pieces, contract):
    block_width = hidden.shape[-1] // pieces
    summed = None
    for part_idx in range(pieces):
        piece_out = jnp.einsum(
            contract,
            hidden[..., part_idx * block_width : (part_idx + 1) * block_width],
            down_rows[..., part_idx * block_width : (part_idx + 1) * block_width, :],
            preferred_element_type=jnp.float32,
        )
        summed = rounded(piece_out) if summed is None else summed + rounded(piece_out)
    return summed.astype(jnp.bfloat16)


def per_device(
    mix_input,
    mix_gain,
    pool_weight,
    pool_scale,
    moe_input,
    moe_gain,
    expert_ids,
    route_score,
    expert_gate,
    expert_up,
    expert_down,
    shared_gate,
    shared_up,
    shared_down,
):
    normed = rms_norm(mix_input, mix_gain)
    row_count, width_all = normed.shape
    reach_rows = max(WINDOWS) - 1
    before = passed_along(normed[row_count - reach_rows :], ("ep", "tp"), 1)
    offset = lax.axis_index(("ep", "tp")) * row_count
    pooled = window_means(normed, before, offset)
    difference = (pooled - normed.astype(jnp.float32).reshape(row_count, len(WINDOWS), -1)).astype(
        jnp.bfloat16
    )
    mixed_out = jnp.einsum(
        "sgc,gcd->sgd", difference, pool_weight, preferred_element_type=jnp.float32
    )
    mix_output = (mixed_out.reshape(row_count, width_all) * pool_scale).astype(jnp.bfloat16)
    h_moe = rms_norm(moe_input, moe_gain)
    tok_count, model_width = h_moe.shape
    top_count = expert_ids.shape[1]
    quarters = lax.axis_size("tp")
    my_quarter = lax.axis_index("tp")
    ep_count = lax.axis_size("ep")
    local_experts = expert_gate.shape[0]
    expert_count = ep_count * local_experts
    capacity = 3 * tok_count * top_count // (2 * expert_count)
    per_source = local_experts * capacity
    full_gate, full_up, full_down, full_sgate, full_sup, full_sdown = (
        *in_one_piece((expert_gate, expert_up), "tp", 2, 0),
        lax.all_gather(expert_down, "tp", axis=1, tiled=True),
        *in_one_piece((shared_gate, shared_up), "tp", 1, 0),
        lax.all_gather(shared_down, "tp", axis=0, tiled=True),
    )
    my_ids = lax.dynamic_slice_in_dim(expert_ids, my_quarter * tok_count, tok_count, 0)
    outgoing, my_slots = fill_slots(h_moe, my_ids, expert_count, capacity)
    landed = lax.all_to_all(
        outgoing.reshape(ep_count, per_source, model_width),
        "ep",
        split_axis=0,
        concat_axis=0,
        tiled=True,
    )
    routed_in = landed.reshape(ep_count, local_experts, capacity, model_width)
    gate_val = jnp.einsum(
        "necd,edf->necf", routed_in, full_gate, preferred_element_type=jnp.float32
    )
    up_val = jnp.einsum("necd,edf->necf", routed_in, full_up, preferred_element_type=jnp.float32)
    hidden = (jax.nn.silu(gate_val) * up_val).astype(jnp.bfloat16)
    expert_back = blockwise_down(hidden, full_down, quarters, "necf,efd->necd")
    expert_back = expert_back.reshape(ep_count, per_source, model_width)
    shared_gate_val = jnp.dot(h_moe, full_sgate, preferred_element_type=jnp.float32)
    shared_up_val = jnp.dot(h_moe, full_sup, preferred_element_type=jnp.float32)
    shared_hidden = (jax.nn.silu(shared_gate_val) * shared_up_val).astype(jnp.bfloat16)
    shared_back = blockwise_down(shared_hidden, full_sdown, quarters, "tf,fd->td")
    returned = lax.all_to_all(expert_back, "ep", split_axis=0, concat_axis=0, tiled=True)
    returned = returned.reshape(expert_count * capacity, model_width)
    route_w = route_score / jnp.sum(route_score, axis=1, keepdims=True) * ROUTED_SCALE
    combined = shared_back.astype(jnp.float32)
    for pick_idx in range(top_count):
        combined = combined + route_w[:, pick_idx : pick_idx + 1] * returned[
            my_slots[:, pick_idx]
        ].astype(jnp.float32)
    return (mix_output, combined.astype(jnp.bfloat16))


def solution(mesh):
    return jax.shard_map(
        per_device,
        mesh=mesh,
        in_specs=(
            P(("ep", "tp"), None),
            P(),
            P(),
            P(),
            P(("ep", "tp"), None),
            P(),
            P("ep", None),
            P(("ep", "tp"), None),
            P("ep", None, "tp"),
            P("ep", None, "tp"),
            P("ep", "tp", None),
            P(None, "tp"),
            P(None, "tp"),
            P("tp", None),
        ),
        out_specs=(P(("ep", "tp"), None), P(("ep", "tp"), None)),
        check_vma=False,
    )
```

profile of v0, /device:TPU:160, one launch (start us, length us, event | category | flops | bytes accessed | tf_op | source)
XLA Modules:
  0.0 439.3 jit_solution(3366335373749575262)
XLA Ops:
  7.2 4.7 %pad_maximum_fusion = bf16[4,2048,256]{2,1,0:T(8,128)(2,1)} fusion(bf16[2,2048,256]{2,1,0:T(8,128)(2,1)} %param.23, bf16[2,2048,256]{2,1,0:T(8,128)(2,1)} %param.22), kind=kLoop, calls=%fused_computation.11 | loop fusion | flops 2097152 | bytes 8388608 | tf_op jit(solution)/shard_map/concatenate | solution.py:22
  14.2 2.4 scatter_custom_fusion
  17.9 4.3 gather_fusion
  22.2 6.2 %reshape.104 = bf16[64,12,2048]{2,1,0:T(8,128)(2,1)} reshape(bf16[768,2048]{1,0:T(8,128)(2,1)} %gather_fusion) | data formatting | bytes 6291456 | tf_op jit(solution)/shard_map/reshape | solution.py:134
  28.5 10.4 %all-to-all-start = ((bf16[64,12,2048]{2,1,0:T(8,128)(2,1)}), bf16[64,12,2048]{2,1,0:T(8,128)(2,1)}, u32[]{:S(2)}, u32[]{:S(2)}) async-start(bf16[64,12,2048]{2,1,0:T(8,128)(2,1)} %reshape.104), calls=%async_computation | async-start | bytes 8388608 | tf_op jit(solution)/shard_map/all_to_all | solution.py:133
  40.2 89.7 %all-to-all-done = bf16[64,12,2048]{2,1,0:T(8,128)(2,1)} async-done(((bf16[64,12,2048]{2,1,0:T(8,128)(2,1)}), bf16[64,12,2048]{2,1,0:T(8,128)(2,1)}, u32[]{:S(2)}, u32[]{:S(2)}) %all-to-all-start) | async-done | bytes 3145760 | tf_op jit(solution)/shard_map/all_to_all | solution.py:133
  129.9 5.6 %copy.28 = bf16[64,12,2048]{2,0,1:T(8,128)(2,1)} copy(bf16[64,12,2048]{2,1,0:T(8,128)(2,1)} %all-to-all-done) | data formatting | bytes 6291456 | tf_op jit(solution)/shard_map/all_to_all | solution.py:133
  135.5 38.0 %all-gather.9.cloned.1.call-done = bf16[4,2048,1024]{2,1,0:T(8,128)(2,1)} async-done(((bf16[4,2048,256]{2,1,0:T(8,128)(2,1)}), bf16[4,2048,1024]{2,1,0:T(8,128)(2,1)}) %all-gather.9.cloned.1.call-update) | async-done | bytes 16777232 | tf_op jit(solution)/shard_map/all_gather | solution.py:23
  173.6 9.3 %fusion = f32[2,1024,64,6]{1,2,3,0:T(8,128)} fusion(bf16[64,2,6,2048]{3,0,2,1:T(8,128)(2,1)} %bitcast.96, bf16[4,2048,1024]{2,1,0:T(8,128)(2,1)} %all-gather.9.cloned.1.call-done), kind=kOutput, calls=%fused_computation.7 | convolution fusion | flops 3221225472 | bytes 14680064 | tf_op jit(solution)/shard_map/necd,edf->necf/dot_general | solution.py:144
  182.9 10.7 %fusion.2 = bf16[64,2,6,1024]{3,0,2,1:T(8,128)(2,1)} fusion(f32[2,1024,64,6]{1,2,3,0:T(8,128)} %fusion, bf16[64,2,6,2048]{3,0,2,1:T(8,128)(2,1)} %bitcast.97, bf16[4,2048,1024]{2,1,0:T(8,128)(2,1)} %all-gather.9.cloned.1.call-done), kind=kOutput, calls=%fused_computation.17 | convolution fusion | flops 3225944064 | bytes 16252928 | tf_op jit(solution)/shard_map/necd,edf->necf/dot_general | solution.py:141
  193.6 67.8 %all-gather.11.cloned.1.call-done = bf16[2,1024,2048]{2,1,0:T(8,128)(2,1)} async-done(((bf16[2,256,2048]{2,1,0:T(8,128)(2,1)}), bf16[2,1024,2048]{2,1,0:T(8,128)(2,1)}) %all-gather.11.cloned.1.call-update) | async-done | bytes 8388624 | tf_op jit(solution)/shard_map/all_gather | solution.py:127
  261.4 2.9 fusion.6
  264.2 3.0 fusion.7
  269.5 3.2 add_convert_fusion
  272.7 3.7 copy.29
  276.5 10.6 %all-to-all-start.1 = ((bf16[64,12,2048]{2,1,0:T(8,128)(2,1)}), bf16[64,12,2048]{2,1,0:T(8,128)(2,1)}, u32[]{:S(2)}, u32[]{:S(2)}) async-start(bf16[64,12,2048]{2,1,0:T(8,128)(2,1)} %copy.29), calls=%async_computation.1 | async-start | bytes 8388608 | tf_op jit(solution)/shard_map/all_to_all | solution.py:152
  287.5 2.9 fusion.62
  290.4 3.6 collective-permute-start
  294.4 88.7 %collective-permute-done = bf16[15,2048]{1,0:T(8,128)(2,1)S(1)} collective-permute-done((bf16[15,2048]{1,0:T(8,128)(2,1)S(1)}, bf16[15,2048]{1,0:T(8,128)(2,1)S(1)}, u32[]{:S(2)}, u32[]{:S(2)}) %collective-permute-start) | collective-permute-done | bytes 61472 | tf_op jit(solution)/shard_map/ppermute | solution.py:14
  387.5 2.9 copy.26
  393.8 2.3 fusion.16
  396.1 2.0 fusion.22
  398.2 2.1 convolution_convert_fusion.7
  400.3 2.1 convolution_convert_fusion.6
  402.4 2.1 convolution_convert_fusion.5
  404.5 2.1 convolution_convert_fusion.4
  406.7 6.2 %reshape.107 = bf16[768,2048]{1,0:T(8,128)(2,1)} reshape(bf16[64,12,2048]{2,1,0:T(8,128)(2,1)} %all-to-all-done.1) | data formatting | bytes 6291456 | tf_op jit(solution)/shard_map/reshape | solution.py:153
  412.8 3.7 gather_fusion.1
  416.6 3.7 gather_fusion.2
  420.3 4.5 %gather_fusion.3 = bf16[128,2048]{1,0:T(8,128)(2,1)} fusion(bf16[768,2048]{1,0:T(8,128)(2,1)} %reshape.107, s32[1024]{0:T(1024)S(1)} %get-tuple-element.26), kind=kCustom, calls=%fused_computation.3 | custom fusion | bytes 1049088 | tf_op jit(solution)/shard_map/gather | solution.py:157
  424.8 4.5 %gather_fusion.4 = bf16[128,2048]{1,0:T(8,128)(2,1)} fusion(bf16[768,2048]{1,0:T(8,128)(2,1)} %reshape.107, s32[1024]{0:T(1024)S(1)} %get-tuple-element.25), kind=kCustom, calls=%fused_computation.4 | custom fusion | bytes 1049088 | tf_op jit(solution)/shard_map/gather | solution.py:157
  429.4 3.4 add_convert_fusion.1
  (75 shorter events, 15.5 us)
Async XLA Ops:
  7.2 377.5 %copy-start = (bf16[4,512,512]{2,1,0:T(8,128)(2,1)S(1)}, bf16[4,512,512]{2,1,0:T(8,128)(2,1)}, u32[]{:S(2)}) copy-start(bf16[4,512,512]{2,1,0:T(8,128)(2,1)} %param.16) | copy-start | bytes 6291460
  7.2 166.4 %all-gather.9.cloned.1.call-start = ((), (), s32[]{:S(2)}) async-start(), calls=%async_computation.4 | async-start | bytes 20971520 | tf_op jit(solution)/shard_map/all_gather | solution.py:23
  11.9 4.7 %copy-start.4 = (bf16[128,2048]{1,0:T(8,128)(2,1)S(1)}, bf16[128,2048]{1,0:T(8,128)(2,1)}, u32[]{:S(2)}) copy-start(bf16[128,2048]{1,0:T(8,128)(2,1)} %param.18) | copy-start | bytes 1572868
  11.9 5.0 %copy-start.10 = (f32[2048]{0:T(1024)S(1)}, f32[2048]{0:T(1024)}, u32[]{:S(2)}) copy-start(f32[2048]{0:T(1024)} %param.19) | copy-start | bytes 24580
  11.9 249.5 %all-gather.11.cloned.1.call-start = ((), (), s32[]{:S(2)}) async-start(), calls=%async_computation.5 | async-start | bytes 10485760 | tf_op jit(solution)/shard_map/all_gather | solution.py:127
  17.0 0.8 copy-start.5
  28.4 10.6 %copy-start.8 = (bf16[2048,128]{1,0:T(8,128)(2,1)S(1)}, bf16[2048,128]{1,0:T(8,128)(2,1)}, u32[]{:S(2)}) copy-start(bf16[2048,128]{1,0:T(8,128)(2,1)} %param.26) | copy-start | bytes 1572868
  28.5 10.6 %copy-start.9 = (bf16[2048,128]{1,0:T(8,128)(2,1)S(1)}, bf16[2048,128]{1,0:T(8,128)(2,1)}, u32[]{:S(2)}) copy-start(bf16[2048,128]{1,0:T(8,128)(2,1)} %param.25) | copy-start | bytes 1572868
  28.5 101.5 %all-to-all-start = ((bf16[64,12,2048]{2,1,0:T(8,128)(2,1)}), bf16[64,12,2048]{2,1,0:T(8,128)(2,1)}, u32[]{:S(2)}, u32[]{:S(2)}) async-start(bf16[64,12,2048]{2,1,0:T(8,128)(2,1)} %reshape.104), calls=%async_computation | async-start | bytes 8388608 | tf_op jit(solution)/shard_map/all_to_all | solution.py:133
  38.8 355.0 %all-gather.5.cloned.1.call-start = ((), (), s32[]{:S(2)}) async-start(), calls=%async_computation.2 | async-start | bytes 5242880 | tf_op jit(solution)/shard_map/all_gather | solution.py:23
  261.4 5.9 %copy-start.2 = (bf16[2,1024,2048]{2,1,0:T(8,128)(2,1)S(1)}, bf16[2,1024,2048]{2,1,0:T(8,128)(2,1)}, u32[]{:S(2)}) copy-start(bf16[2,1024,2048]{2,1,0:T(8,128)(2,1)} %all-gather.11.cloned.1.call-done) | copy-start | bytes 25165828
  264.2 3.0 copy-start.7
  276.5 10.7 %copy-start.3 = (bf16[256,2048]{1,0:T(8,128)(2,1)S(1)}, bf16[256,2048]{1,0:T(8,128)(2,1)}, u32[]{:S(2)}) copy-start(bf16[256,2048]{1,0:T(8,128)(2,1)} %param.14) | copy-start | bytes 3145732
  276.5 11.0 %copy-start.11 = (f32[2048]{0:T(1024)S(1)}, f32[2048]{0:T(1024)}, u32[]{:S(2)}) copy-start(f32[2048]{0:T(1024)} %param.15) | copy-start | bytes 24580
  276.5 130.2 %all-to-all-start.1 = ((bf16[64,12,2048]{2,1,0:T(8,128)(2,1)}), bf16[64,12,2048]{2,1,0:T(8,128)(2,1)}, u32[]{:S(2)}, u32[]{:S(2)}) async-start(bf16[64,12,2048]{2,1,0:T(8,128)(2,1)} %copy.29), calls=%async_computation.1 | async-start | bytes 8388608 | tf_op jit(solution)/shard_map/all_to_all | solution.py:152
  287.1 6.9 %copy-start.13 = (f32[128,4]{0,1:T(4,128)S(1)}, f32[128,4]{0,1:T(4,128)}, u32[]{:S(2)}) copy-start(f32[128,4]{0,1:T(4,128)} %param.21) | copy-start | bytes 6148
  287.1 111.0 %all-gather.7.cloned.1.call-start = ((), (), s32[]{:S(2)}) async-start(), calls=%async_computation.3 | async-start | bytes 2621440 | tf_op jit(solution)/shard_map/all_gather | solution.py:129
  290.4 92.7 %collective-permute-start = (bf16[15,2048]{1,0:T(8,128)(2,1)S(1)}, bf16[15,2048]{1,0:T(8,128)(2,1)S(1)}, u32[]{:S(2)}, u32[]{:S(2)}) collective-permute-start(bf16[15,2048]{1,0:T(8,128)(2,1)S(1)} %slice.264), channel_id=1, source_target_pairs={{0,1},{1,2},{2,3},{3,4},{4,5},{5,6},{6,7},{7,8},{8,9},{9,10},{10,1... | collective-permute-start | bytes 184328 | tf_op jit(solution)/shard_map/ppermute | solution.py:14
  383.9 1.6 copy-start.1
  387.5 2.9 copy-start.12
  393.8 2.3 copy-start.6
Sparse Core Ops, SparseCore 0:
  12.0 161.4 all-gather.8
  175.4 85.9 all-gather.10
  263.2 56.2 all-gather.4
  321.2 33.6 all-gather.6
where the time goes:
time: 440 us; the launch traced here: 439 us
  waiting for transfers between devices  285 us (65%)
  local copies, waits for them, and re-layouts  52.3 us (12%)
  matrix products  43.2 us (10%)
  starting transfers between devices  25 us (6%)
  other arithmetic  19.6 us (4%)
  between operations  14.2 us (3%)
    all_to_all x1, waiting for transfers between devices, per_device(): lax.all_to_all(outgoing.reshape(ep_count, per_source, model_width), 'ep',...  89.7 us
    ppermute x1, waiting for transfers between devices, passed_along(): return lax.ppermute(value, axis, pairs)  88.7 us
    all_gather x1, waiting for transfers between devices, per_device(): lax.all_gather(expert_down, 'tp', axis=1, tiled=True)  67.8 us
    all_gather x2, waiting for transfers between devices, in_one_piece(): lax.all_gather(both, axis, axis=dim, tiled=True)  38 us
    dot_general x8, matrix products, blockwise_down(): jnp.einsum(contract, hidden[..., part_idx * block_width:(part_idx + 1) *...  16.6 us
    gather x4, local copies, waits for them, and re-layouts, per_device(): returned[my_slots[:, pick_idx]].astype(jnp.float32)  16.5 us
    dot_general x1, matrix products, per_device(): jnp.einsum('necd,edf->necf', routed_in, full_gate, preferred_element_type...  10.7 us
    all_to_all x1, starting transfers between devices, per_device(): lax.all_to_all(expert_back, 'ep', split_axis=0, concat_axis=0, tiled=True)  10.6 us
  transfers between devices with their start and end apart: 7, of which 4 were waited for; matrix products, arithmetic and copies ran while one was open for 19% of the time, Pallas kernels for 0%

commit v1 on v0

v1 whole, which is shorter than its diff:
```python
import jax
import jax.numpy as jnp
import numpy as np
from jax import lax
from jax.experimental import pallas as pl
from jax.experimental.pallas import tpu as pltpu
from jax.sharding import PartitionSpec as P


WINDOWS = (2, 4, 8, 16)
RMS_EPS = 1e-06
ROUTED_SCALE = 2.5
CAP = 6
COLS = 4
PACK = CAP * COLS
BLOCK = 8
PAIR_A = ((0, 1), (1, 0), (2, 3), (3, 2))
PAIR_B = ((1, 2), (2, 1), (3, 0), (0, 3))


f32 = jnp.float32
bf16 = jnp.bfloat16


def dot32(a, b):
    return jnp.dot(a, b, preferred_element_type=f32)


def call(body, out, scratch=(), smem=(), count=0, plane=None):
    def spec(i):
        if plane and i in plane:
            at, shape = plane[i]
            return pl.BlockSpec((None, *shape), lambda _: (at, 0, 0))
        return pl.BlockSpec(memory_space=pltpu.SMEM if i in smem else pltpu.VMEM)

    return pl.pallas_call(
        body,
        out_shape=out,
        grid=(1,) if plane else (),
        in_specs=[spec(i) for i in range(count)],
        scratch_shapes=list(scratch),
    )


def unpack_matrix():
    rows = BLOCK * PACK
    per = BLOCK * CAP
    place = np.zeros((rows, rows), np.float32)
    for i in range(rows):
        q, rest = divmod(i, per)
        j, s = divmod(rest, CAP)
        place[i, j * PACK + q * CAP + s] = 1.0
    return place


def dispatch_body(x_ref, gain_ref, ids_ref, h_ref, m0_ref, m1_ref, rank_ref, hcat_ref):
    x = x_ref[...].astype(f32)
    mean = jnp.mean(x * x, axis=-1, keepdims=True)
    h = (x * lax.rsqrt(mean + RMS_EPS) * gain_ref[...]).astype(bf16)
    h_ref[...] = h
    toks, width = h.shape
    part = width // COLS
    for q in range(COLS):
        hcat_ref[q * toks : (q + 1) * toks, :] = h[:, q * part : (q + 1) * part]
    peers = rank_ref.shape[0]
    before = (
        lax.broadcasted_iota(jnp.int32, (toks, toks), 0)
        < lax.broadcasted_iota(jnp.int32, (toks, toks), 1)
    ).astype(f32).astype(bf16)
    for e, m_ref in enumerate((m0_ref, m1_ref)):
        expert = 2 * lax.broadcasted_iota(jnp.int32, (peers, toks), 0) + e
        named = jnp.zeros((peers, toks), f32)
        for k in range(ids_ref.shape[0]):
            named = named + (ids_ref[k : k + 1, :] == expert).astype(f32)
        rank = dot32(named.astype(bf16), before)
        rank = jnp.where(named > 0, rank, -1.0)
        for q in range(COLS):
            rank_ref[:, q * toks : (q + 1) * toks] = rank

        def block(b, _):
            ranks = rank_ref[pl.ds(pl.multiple_of(b * BLOCK, BLOCK), BLOCK), :]
            shape = (BLOCK, PACK, COLS * toks)
            r = lax.broadcasted_iota(jnp.int32, shape, 1)
            col = lax.broadcasted_iota(jnp.int32, shape, 2)
            q = sum((r >= CAP * i).astype(jnp.int32) for i in range(1, COLS))
            want = jnp.where(
                (col >= q * toks) & (col < (q + 1) * toks), (r - CAP * q).astype(f32), -2.0
            )
            pick = (jnp.broadcast_to(ranks[:, None, :], shape) == want).astype(f32)
            pick = pick.reshape(BLOCK * PACK, COLS * toks).astype(bf16)
            rows = BLOCK * PACK
            m_ref[pl.ds(pl.multiple_of(b * rows, rows), rows), :] = dot32(
                pick, hcat_ref[...]
            ).astype(bf16)
            return 0

        lax.fori_loop(0, peers // BLOCK, block, 0)


def unpack_into(x_ref, place_ref, rows_ref):
    rows = BLOCK * PACK
    per = BLOCK * CAP
    part = x_ref.shape[1]

    def block(b, _):
        got = dot32(
            place_ref[...], x_ref[pl.ds(pl.multiple_of(b * rows, rows), rows), :]
        ).astype(bf16)
        for q in range(COLS):
            rows_ref[
                pl.ds(pl.multiple_of(b * per, per), per), q * part : (q + 1) * part
            ] = got[q * per : (q + 1) * per, :]
        return 0

    lax.fori_loop(0, x_ref.shape[0] // rows, block, 0)


def hidden_body(x_ref, place_ref, ga_ref, ua_ref, gb_ref, ub_ref, hid_ref, rows_ref):
    unpack_into(x_ref, place_ref, rows_ref)
    x = rows_ref[...]
    w = ga_ref.shape[-1]
    for i, (g_ref, u_ref) in enumerate(((ga_ref, ua_ref), (gb_ref, ub_ref))):
        gate = dot32(x, g_ref[...])
        up = dot32(x, u_ref[...])
        hid_ref[:, i * w : (i + 1) * w] = (gate / (1.0 + jnp.exp(-gate)) * up).astype(bf16)


def down_body(mine_ref, theirs_ref, d0_ref, d1_ref, d2_ref, d3_ref, place_ref, out_ref, y_ref):
    w = mine_ref.shape[1] // 2
    total = dot32(mine_ref[:, :w], d0_ref[...]) + dot32(mine_ref[:, w:], d1_ref[...])
    total = total + dot32(theirs_ref[:, :w], d2_ref[...]) + dot32(theirs_ref[:, w:], d3_ref[...])
    y_ref[...] = total.astype(bf16)
    rows = BLOCK * PACK
    per = BLOCK * CAP
    part = out_ref.shape[1]

    def block(b, _):
        at = pl.ds(pl.multiple_of(b * per, per), per)
        stack = jnp.concatenate(
            [y_ref[at, q * part : (q + 1) * part] for q in range(COLS)], axis=0
        )
        out_ref[pl.ds(pl.multiple_of(b * rows, rows), rows), :] = dot32(
            place_ref[...], stack
        ).astype(bf16)
        return 0

    lax.fori_loop(0, y_ref.shape[0] // per, block, 0)


def combine_body(e, ids_ref, score_ref, base_ref, r_ref, place_ref, out_ref, rows_ref):
    unpack_into(r_ref, place_ref, rows_ref)
    toks = ids_ref.shape[0]
    total = rows_ref.shape[0]
    peers = total // CAP
    score = score_ref[...]
    weight = score / jnp.sum(score, axis=1, keepdims=True) * ROUTED_SCALE
    expert = 2 * lax.broadcasted_iota(jnp.int32, (toks, peers), 1) + e
    named = jnp.zeros((toks, peers), f32)
    scaled = jnp.zeros((toks, peers), f32)
    for k in range(ids_ref.shape[1]):
        hit = ids_ref[:, k : k + 1] == expert
        named = named + hit.astype(f32)
        scaled = scaled + jnp.where(hit, weight[:, k : k + 1], 0.0)
    before = (
        lax.broadcasted_iota(jnp.int32, (toks, toks), 1)
        < lax.broadcasted_iota(jnp.int32, (toks, toks), 0)
    ).astype(f32).astype(bf16)
    rank = jnp.where(named > 0, dot32(before, named.astype(bf16)), -1.0).astype(bf16)
    at = lax.broadcasted_iota(jnp.int32, (peers, total), 1) - CAP * lax.broadcasted_iota(
        jnp.int32, (peers, total), 0
    )
    mine = (at >= 0) & (at < CAP)
    spread = mine.astype(f32).astype(bf16)
    slot = jnp.sum(jnp.where(mine, at, 0).astype(f32), axis=0, keepdims=True)
    here = dot32(rank, spread) == slot
    high = scaled.astype(bf16)
    low = (scaled - high.astype(f32)).astype(bf16)
    acc = base_ref[...].astype(f32)
    for piece in (high, low):
        lhs = jnp.where(here, dot32(piece, spread), 0.0).astype(bf16)
        acc = acc + dot32(lhs, rows_ref[...])
    out_ref[...] = acc.astype(out_ref.dtype)


def rms_norm(values, gain_row):
    upcast = values.astype(f32)
    scaled = upcast * lax.rsqrt(jnp.mean(upcast * upcast, axis=-1, keepdims=True) + RMS_EPS)
    return (scaled * gain_row).astype(bf16)


def mixer_body(at_ref, x_ref, gain_ref, halo_ref, pool_ref, scale_ref, out_ref, rows_ref):
    lead = halo_ref.shape[0]
    rows, width = x_ref.shape
    group = width // len(WINDOWS)
    rows_ref[:lead, :] = halo_ref[...]
    rows_ref[lead:, :] = rms_norm(x_ref[...], gain_ref[...])
    ahead = lax.broadcasted_iota(jnp.int32, (rows, lead + rows), 0) + lead
    back = ahead - lax.broadcasted_iota(jnp.int32, (rows, lead + rows), 1)
    taken = at_ref[0] + 1 + lax.broadcasted_iota(jnp.int32, (rows, 1), 0)
    for g, span in enumerate(WINDOWS):
        cols = slice(g * group, (g + 1) * group)
        band = ((back >= 0) & (back < span)).astype(f32).astype(bf16)
        pooled = dot32(band, rows_ref[:, cols]) / jnp.minimum(taken, span).astype(f32)
        difference = (pooled - rows_ref[lead:, cols].astype(f32)).astype(bf16)
        out_ref[:, cols] = (dot32(difference, pool_ref[g]) * scale_ref[:, cols]).astype(bf16)


def tail_before(mix_input, mix_gain):
    lead = max(WINDOWS)
    length = lax.axis_size(("ep", "tp"))
    return lax.ppermute(
        rms_norm(mix_input[mix_input.shape[0] - lead :], mix_gain),
        ("ep", "tp"),
        [(i, i + 1) for i in range(length - 1)],
    )


def mixer(mix_input, mix_gain, before, pool_weight, pool_scale):
    rows, width = mix_input.shape
    lead = before.shape[0]
    offset = (lax.axis_index(("ep", "tp")) * rows).astype(jnp.int32)
    return call(
        mixer_body,
        jax.ShapeDtypeStruct((rows, width), bf16),
        (pltpu.VMEM((lead + rows, width), bf16),),
        smem=(0,),
        count=6,
    )(offset[None], mix_input, mix_gain[None, :], before, pool_weight, pool_scale[None, :])


def layer(
    mix_input,
    mix_gain,
    pool_weight,
    pool_scale,
    moe_input,
    moe_gain,
    expert_ids,
    route_score,
    expert_gate,
    expert_up,
    expert_down,
    shared_gate,
    shared_up,
    shared_down,
):
    toks, width = moe_input.shape
    peers = lax.axis_size("ep")
    quarter = lax.axis_index("tp")
    part = width // COLS
    packed = peers * PACK
    slots = peers * CAP
    place = jnp.asarray(unpack_matrix(), bf16)
    place_back = jnp.asarray(unpack_matrix().T, bf16)
    my_ids = lax.dynamic_slice_in_dim(expert_ids, quarter * toks, toks, 0)

    pairs = (PAIR_A, PAIR_B)

    def swap(value, pairs):
        return lax.ppermute(value, "tp", pairs)

    pairs = (PAIR_A, PAIR_B)
    gates = [swap(expert_gate[e], pairs[e]) for e in range(2)]
    ups = [swap(expert_up[e], pairs[e]) for e in range(2)]
    down_a = swap(expert_down, PAIR_A)
    down_b = [swap(expert_down[e], PAIR_B) for e in range(2)]
    across = [swap(down_b[0], PAIR_A), swap(down_a[1], PAIR_B)]

    h, *sends = call(
        dispatch_body,
        (
            jax.ShapeDtypeStruct((toks, width), bf16),
            jax.ShapeDtypeStruct((packed, part), bf16),
            jax.ShapeDtypeStruct((packed, part), bf16),
        ),
        (pltpu.VMEM((peers, COLS * toks), f32), pltpu.VMEM((COLS * toks, part), bf16)),
        count=3,
    )(moe_input, moe_gain[None, :], my_ids.T)

    def over_ep(value):
        value = value.reshape(peers, PACK, part)
        return lax.all_to_all(value, "ep", 0, 0, tiled=True).reshape(packed, part)

    def hidden_half(rows, e):
        return call(
            hidden_body,
            jax.ShapeDtypeStruct((slots, 2 * expert_gate.shape[2]), bf16),
            (pltpu.VMEM((slots, width), bf16),),
            count=6,
            plane={i: (e, expert_gate.shape[1:]) for i in (2, 3)},
        )(rows, place, expert_gate, expert_up, gates[e], ups[e])

    back = []
    for e in range(2):
        own = over_ep(sends[e])
        other = swap(own, pairs[1 - e])
        mine = hidden_half(own, e)
        theirs = hidden_half(other, e)
        theirs = swap(theirs, pairs[1 - e])
        whole = (e, expert_down.shape[1:])
        weights = (expert_down, down_a, down_b[0], across[0])
        planes = {2: whole, 3: whole}
        if e == 1:
            weights = (expert_down, down_b[1], down_a, across[1])
            planes = {2: whole, 4: whole}
        back.append(
            call(
                down_body,
                jax.ShapeDtypeStruct((packed, part), bf16),
                (pltpu.VMEM((slots, width), bf16),),
                count=7,
                plane=planes,
            )(mine, theirs, *weights, place_back)
        )

    everyone = lax.all_gather(h, "tp", axis=0, tiled=True)
    shared_hidden = (
        jax.nn.silu(dot32(everyone, shared_gate)) * dot32(everyone, shared_up)
    ).astype(bf16)
    shared_part = dot32(shared_hidden, shared_down).astype(bf16)
    acc = lax.psum_scatter(shared_part, "tp", scatter_dimension=0, tiled=True)

    halo = tail_before(mix_input, mix_gain)
    mix_output = mixer(mix_input, mix_gain, halo, pool_weight, pool_scale)

    for e in range(2):
        returned = over_ep(back[e])
        acc = call(
            lambda *refs, e=e: combine_body(e, *refs),
            jax.ShapeDtypeStruct((toks, width), bf16 if e == 1 else f32),
            (pltpu.VMEM((slots, width), bf16),),
            count=5,
        )(my_ids, route_score, acc, returned, place)
    return (mix_output, acc)


def solution(mesh):
    return jax.shard_map(
        layer,
        mesh=mesh,
        in_specs=(
            P(("ep", "tp"), None),
            P(),
            P(),
            P(),
            P(("ep", "tp"), None),
            P(),
            P("ep", None),
            P(("ep", "tp"), None),
            P("ep", None, "tp"),
            P("ep", None, "tp"),
            P("ep", "tp", None),
            P(None, "tp"),
            P(None, "tp"),
            P("tp", None),
        ),
        out_specs=(P(("ep", "tp"), None), P(("ep", "tp"), None)),
        check_vma=False,
    )
```

time: 440 us -> 419 us (0.952)
  Pallas kernels: 0 us -> 64.8 us
  waiting for transfers between devices: 285 us -> 221 us
  blocking collectives: 0 us -> 47.3 us
  local copies, waits for them, and re-layouts: 52.3 us -> 14.3 us
  matrix products: 43.2 us -> 7.13 us
  starting transfers between devices: 25 us -> 47.9 us
  other arithmetic: 19.6 us -> 1.9 us
    ppermute x1 -> x14, waiting for transfers between devices: 88.7 us -> 221 us  [the longest x13 185 us: swap(): return lax.ppermute(value, 'tp', pairs)]
    all_gather x4 -> x1, waiting for transfers between devices: 106 us -> 0.01 us  [layer(): everyone = lax.all_gather(h, 'tp', axis=0, tiled=True)]
    all_to_all x2 -> x3, waiting for transfers between devices: 89.7 us -> 0.01 us  [over_ep(): return lax.all_to_all(value, 'ep', 0, 0, tiled=True).reshape(packed, part)]
    pallas_call x0 -> x10, Pallas kernels: none -> 64.8 us  [the longest x4 27.6 us: hidden_half(): call(hidden_body, jax.ShapeDtypeStruct((slots, 2 * expert_gate.shape[2]),...]
    all_to_all x0 -> x1, blocking collectives: none -> 47.3 us  [over_ep(): return lax.all_to_all(value, 'ep', 0, 0, tiled=True).reshape(packed, part)]
    dot_general x14 -> x2, matrix products: 43.2 us -> 7.13 us  [dot32(): return jnp.dot(a, b, preferred_element_type=f32)]
    gather x5 -> x0, local copies, waits for them, and re-layouts: 20.9 us -> none  [the longest x4 16.5 us: per_device(): returned[my_slots[:, pick_idx]].astype(jnp.float32)]
    reshape x3 -> x0, local copies, waits for them, and re-layouts: 16.1 us -> none  [the longest x1 6.2 us: per_device(): outgoing.reshape(ep_count, per_source, model_width)]
  transfers between devices with their start and end apart: 7 -> 19, of which waited for: 4 -> 9; matrix products, arithmetic and copies ran while one was open for 19% -> 4% of each run, Pallas kernels for 0% -> 12%
where the time goes in v1:
time: 419 us; the launch traced here: 418 us
  waiting for transfers between devices  221 us (53%)
  Pallas kernels  64.8 us (15%)
  starting transfers between devices  47.9 us (11%)
  blocking collectives  47.3 us (11%)
  local copies, waits for them, and re-layouts  14.3 us (3%)
  between operations  14.2 us (3%)
  matrix products  7.13 us (2%)
    ppermute x13, waiting for transfers between devices, swap(): return lax.ppermute(value, 'tp', pairs)  185 us
    all_to_all x1, blocking collectives, over_ep(): return lax.all_to_all(value, 'ep', 0, 0, tiled=True).reshape(packed, part)  47.3 us
    ppermute x1, waiting for transfers between devices, tail_before(): lax.ppermute(rms_norm(mix_input[mix_input.shape[0] - lead:], mix_gain), (...  35.9 us
    all_to_all x3, starting transfers between devices, over_ep(): return lax.all_to_all(value, 'ep', 0, 0, tiled=True).reshape(packed, part)  29.5 us
    pallas_call x4, Pallas kernels, hidden_half(): call(hidden_body, jax.ShapeDtypeStruct((slots, 2 * expert_gate.shape[2]),...  27.6 us
    ppermute x13, starting transfers between devices, swap(): return lax.ppermute(value, 'tp', pairs)  15.9 us
    pallas_call x2, Pallas kernels, layer(): call(down_body, jax.ShapeDtypeStruct((packed, part), bf16), (pltpu.VMEM((...  14.2 us
    pallas_call x2, Pallas kernels, layer(): call(lambda *refs, e=e: combine_body(e, *refs), jax.ShapeDtypeStruct((tok...  11 us
  transfers between devices with their start and end apart: 19, of which 9 were waited for; matrix products, arithmetic and copies ran while one was open for 4% of the time, Pallas kernels for 12%

profile of v1, /device:TPU:160, one launch (start us, length us, event | category | flops | bytes accessed | tf_op | source)
XLA Modules:
  0.0 418.3 jit_solution(13393134280537520790)
XLA Ops:
  8.7 7.3 %shard_map.168 = (bf16[128,2048]{1,0:T(8,128)(2,1)}, bf16[1536,512]{1,0:T(8,128)(2,1)}, bf16[1536,512]{1,0:T(8,128)(2,1)}) custom-call(bf16[128,2048]{1,0:T(8,128)(2,1)} %x_ref.3, f32[1,2048]{1,0:T(1,128)} %bitcast.40, s32[4,128]{1,0:T(4,128)} %copy.19.ids_ref), custom_call_target="tpu_custom_call" | custom-call | tf_op jit(solution)/shard_map/pallas_call | solution.py:269
  16.0 47.3 %all_to_all.20 = bf16[64,24,512]{2,1,0:T(8,128)(2,1)} all-to-all(bf16[64,24,512]{2,1,0:T(8,128)(2,1)} %bitcast.37), channel_id=1, replica_groups=mesh['ep'=64,'tp'=4] {'ep'}, dimensions={0} | all-to-all | bytes 3145728 | tf_op jit(solution)/shard_map/all_to_all | solution.py:282
  63.3 8.5 %all-to-all-start.2 = ((bf16[64,24,512]{2,1,0:T(8,128)(2,1)}), bf16[64,24,512]{2,1,0:T(8,128)(2,1)}, u32[]{:S(2)}, u32[]{:S(2)}) async-start(bf16[64,24,512]{2,1,0:T(8,128)(2,1)} %bitcast.12), calls=%async_computation.3 | async-start | bytes 3145728 | tf_op jit(solution)/shard_map/all_to_all | solution.py:282
  71.9 1.6 collective-permute-start.5
  73.5 3.2 slice_bitcast_fusion.1
  76.6 2.1 collective-permute-start.6
  83.6 30.1 %collective-permute-done.6.d2_ref = bf16[256,2048]{1,0:T(8,128)(2,1)} collective-permute-done((bf16[256,2048]{1,0:T(8,128)(2,1)}, bf16[256,2048]{1,0:T(8,128)(2,1)}, u32[]{:S(2)}, u32[]{:S(2)}) %collective-permute-start.6) | collective-permute-done | bytes 1048608 | tf_op jit(solution)/shard_map/ppermute | solution.py:260
  113.8 46.2 %collective-permute-done.1.gb_ref = bf16[2048,256]{1,0:T(8,128)(2,1)S(1)} collective-permute-done((bf16[2048,256]{1,0:T(8,128)(2,1)S(1)}, bf16[2048,256]{1,0:T(8,128)(2,1)S(1)}, u32[]{:S(2)}, u32[]{:S(2)}) %collective-permute-start.1) | collective-permute-done | bytes 1048608 | tf_op jit(solution)/shard_map/ppermute | solution.py:260
  160.0 22.5 %collective-permute-done.2.ub_ref = bf16[2048,256]{1,0:T(8,128)(2,1)S(1)} collective-permute-done((bf16[2048,256]{1,0:T(8,128)(2,1)S(1)}, bf16[2048,256]{1,0:T(8,128)(2,1)S(1)}, u32[]{:S(2)}, u32[]{:S(2)}) %collective-permute-start.2) | collective-permute-done | bytes 1048608 | tf_op jit(solution)/shard_map/ppermute | solution.py:260
  183.4 6.9 %shard_map.170 = bf16[384,512]{1,0:T(8,128)(2,1)} custom-call(bf16[1536,512]{1,0:T(8,128)(2,1)} %collective-permute-done.3.x_ref, bf16[192,192]{1,0:T(8,128)(2,1)} %constant.33.clone.place_ref.refs_4_, bf16[2,2048,256]{2,1,0:T(8,128)(2,1)} %ga_ref.7, bf16[2,2048,256]{2,1,0:T(8,128)(2,1)} %ua_ref.7, bf16[2048,256]{1,0:T(8,128)(2,1)} %copy-done.6, ...), custom_call_target="tpu_custom_call" | custom-call | tf_op jit(solution)/shard_map/pallas_call | solution.py:285
  190.4 2.8 collective-permute-start.4
  193.1 6.9 %shard_map.169.mine_ref = bf16[384,512]{1,0:T(8,128)(2,1)} custom-call(bf16[1536,512]{1,0:T(8,128)(2,1)} %bitcast.34, bf16[192,192]{1,0:T(8,128)(2,1)} %constant.33.clone.place_ref.refs_4_, bf16[2,2048,256]{2,1,0:T(8,128)(2,1)} %ga_ref.7, bf16[2,2048,256]{2,1,0:T(8,128)(2,1)} %ua_ref.7, bf16[2048,256]{1,0:T(8,128)(2,1)} %copy-done.6, bf16[2048,256]{1,0:T(8,128)(2,1)} %copy-done.7), custom_call_target="tpu_custom_call" | custom-call | tf_op jit(solution)/shard_map/pallas_call | solution.py:285
  200.0 4.2 collective-permute-done.7.d3_ref
  205.0 7.1 %shard_map.171 = bf16[1536,512]{1,0:T(8,128)(2,1)} custom-call(bf16[384,512]{1,0:T(8,128)(2,1)} %shard_map.169.mine_ref, bf16[384,512]{1,0:T(8,128)(2,1)} %copy-done.12, bf16[2,256,2048]{2,1,0:T(8,128)(2,1)} %d0_ref.3, bf16[2,256,2048]{2,1,0:T(8,128)(2,1)} %collective-permute-done.5.d1_ref.d2_ref, bf16[256,2048]{1,0:T(8,128)(2,1)} %collective-permute-done.6.d2_ref, ...), custom_call_target="tpu_custom_call" | custom-call | tf_op jit(solution)/shard_map/pallas_call | solution.py:307
  212.1 10.6 %all-to-all-start.1 = ((bf16[64,24,512]{2,1,0:T(8,128)(2,1)}), bf16[64,24,512]{2,1,0:T(8,128)(2,1)}, u32[]{:S(2)}, u32[]{:S(2)}) async-start(bf16[64,24,512]{2,1,0:T(8,128)(2,1)} %bitcast.33), calls=%async_computation.2 | async-start | bytes 3145728 | tf_op jit(solution)/shard_map/all_to_all | solution.py:282
  222.7 2.8 collective-permute-start.8
  226.1 2.8 collective-permute-start.12
  228.8 2.4 fusion.11
  231.3 4.7 %convolution_convert_fusion = bf16[512,2048]{1,0:T(8,128)(2,1)} fusion(bf16[128,2048]{1,0:T(8,128)(2,1)S(1)} %copy-done, bf16[512,2048]{1,0:T(8,128)(2,1)S(1)} %copy-done.3, bf16[2048,128]{1,0:T(8,128)(2,1)} %param.28, f32[512,128]{1,0:T(8,128)S(1)} %fusion.11), kind=kOutput, calls=%fused_computation | convolution fusion | flops 538312704 | bytes 5505024 | tf_op jit(solution)/shard_map/dot_general | solution.py:26
  237.9 13.3 %collective-permute-done.8.gb_ref = bf16[2048,256]{1,0:T(8,128)(2,1)} collective-permute-done((bf16[2048,256]{1,0:T(8,128)(2,1)}, bf16[2048,256]{1,0:T(8,128)(2,1)}, u32[]{:S(2)}, u32[]{:S(2)}) %collective-permute-start.8) | collective-permute-done | bytes 1048608 | tf_op jit(solution)/shard_map/ppermute | solution.py:260
  251.1 38.6 %collective-permute-done.9.ub_ref = bf16[2048,256]{1,0:T(8,128)(2,1)} collective-permute-done((bf16[2048,256]{1,0:T(8,128)(2,1)}, bf16[2048,256]{1,0:T(8,128)(2,1)}, u32[]{:S(2)}, u32[]{:S(2)}) %collective-permute-start.9) | collective-permute-done | bytes 1048608 | tf_op jit(solution)/shard_map/ppermute | solution.py:260
  289.7 6.9 %shard_map.174 = bf16[384,512]{1,0:T(8,128)(2,1)} custom-call(bf16[1536,512]{1,0:T(8,128)(2,1)} %collective-permute-done.10.x_ref, bf16[192,192]{1,0:T(8,128)(2,1)} %constant.33.clone.place_ref.refs_4_, bf16[2,2048,256]{2,1,0:T(8,128)(2,1)} %ga_ref.7, bf16[2,2048,256]{2,1,0:T(8,128)(2,1)} %ua_ref.7, bf16[2048,256]{1,0:T(8,128)(2,1)} %collective-permute-done.8.gb_ref, ...), custom_call_target="tpu_custom_call" | custom-call | tf_op jit(solution)/shard_map/pallas_call | solution.py:285
  296.9 6.9 %shard_map.173.mine_ref = bf16[384,512]{1,0:T(8,128)(2,1)} custom-call(bf16[1536,512]{1,0:T(8,128)(2,1)} %bitcast.13.x_ref, bf16[192,192]{1,0:T(8,128)(2,1)} %constant.33.clone.place_ref.refs_4_, bf16[2,2048,256]{2,1,0:T(8,128)(2,1)} %ga_ref.7, bf16[2,2048,256]{2,1,0:T(8,128)(2,1)} %ua_ref.7, bf16[2048,256]{1,0:T(8,128)(2,1)} %collective-permute-done.8.gb_ref, ...), custom_call_target="tpu_custom_call" | custom-call | tf_op jit(solution)/shard_map/pallas_call | solution.py:285
  303.8 8.4 %collective-permute-done.12.d1_ref = bf16[256,2048]{1,0:T(8,128)(2,1)} collective-permute-done((bf16[256,2048]{1,0:T(8,128)(2,1)}, bf16[256,2048]{1,0:T(8,128)(2,1)}, u32[]{:S(2)}, u32[]{:S(2)}) %collective-permute-start.12) | collective-permute-done | bytes 1048608 | tf_op jit(solution)/shard_map/ppermute | solution.py:260
  312.2 21.5 %collective-permute-done.13.d3_ref = bf16[256,2048]{1,0:T(8,128)(2,1)S(1)} collective-permute-done((bf16[256,2048]{1,0:T(8,128)(2,1)S(1)}, bf16[256,2048]{1,0:T(8,128)(2,1)S(1)}, u32[]{:S(2)}, u32[]{:S(2)}) %collective-permute-start.13) | collective-permute-done | bytes 1048608 | tf_op jit(solution)/shard_map/ppermute | solution.py:260
  335.4 7.0 %shard_map.175 = bf16[1536,512]{1,0:T(8,128)(2,1)} custom-call(bf16[384,512]{1,0:T(8,128)(2,1)} %shard_map.173.mine_ref, bf16[384,512]{1,0:T(8,128)(2,1)} %copy-done.11, bf16[2,256,2048]{2,1,0:T(8,128)(2,1)} %d0_ref.3, bf16[256,2048]{1,0:T(8,128)(2,1)} %collective-permute-done.12.d1_ref, bf16[2,256,2048]{2,1,0:T(8,128)(2,1)} %collective-permute-done.5.d1_ref.d2_ref, ...), custom_call_target="tpu_custom_call" | custom-call | tf_op jit(solution)/shard_map/pallas_call | solution.py:307
  342.5 10.4 %all-to-all-start.3 = ((bf16[64,24,512]{2,1,0:T(8,128)(2,1)}), bf16[64,24,512]{2,1,0:T(8,128)(2,1)S(1)}, u32[]{:S(2)}, u32[]{:S(2)}) async-start(bf16[64,24,512]{2,1,0:T(8,128)(2,1)} %bitcast.36), calls=%async_computation.4 | async-start | bytes 3145728 | tf_op jit(solution)/shard_map/all_to_all | solution.py:282
  354.8 2.4 collective-permute-start
  358.0 35.9 %collective-permute-done.halo_ref = bf16[16,2048]{1,0:T(8,128)(2,1)S(1)} collective-permute-done((bf16[16,2048]{1,0:T(8,128)(2,1)S(1)}, bf16[16,2048]{1,0:T(8,128)(2,1)S(1)}, u32[]{:S(2)}, u32[]{:S(2)}) %collective-permute-start) | collective-permute-done | bytes 65568 | tf_op jit(solution)/shard_map/ppermute | solution.py:211
  394.5 4.7 %shard_map.167 = bf16[256,2048]{1,0:T(8,128)(2,1)} custom-call(s32[1]{0:T(128)} %bitcast.at_ref, bf16[256,2048]{1,0:T(8,128)(2,1)} %x_ref.2, f32[1,2048]{1,0:T(1,128)} %bitcast.39, bf16[16,2048]{1,0:T(8,128)(2,1)} %copy-done.13, bf16[4,512,512]{2,1,0:T(8,128)(2,1)} %pool_ref.1, f32[1,2048]{1,0:T(1,128)} %bitcast.41), custom_call_target="tpu_custom_call" | custom-call | tf_op jit(solution)/shard_map/pallas_call | solution.py:222
  399.2 5.5 %shard_map.172.refs_2_ = f32[128,2048]{1,0:T(8,128)} custom-call(s32[128,4]{1,0:T(8,128)} %copy-done.9, f32[128,4]{1,0:T(8,128)} %copy.21.refs_1_, bf16[128,2048]{1,0:T(8,128)(2,1)} %reduce-scatter.2.cloned.1.call-done.refs_2_, bf16[1536,512]{1,0:T(8,128)(2,1)} %bitcast.11.refs_3_, bf16[192,192]{1,0:T(8,128)(2,1)} %constant.33.clone.place_ref.refs_4_), custom_call_target="tpu_custom_call" | custom-call | tf_op jit(solution)/shard_map/pallas_call | solution.py:328
  405.9 5.5 %shard_map.176 = bf16[128,2048]{1,0:T(8,128)(2,1)} custom-call(s32[128,4]{1,0:T(8,128)} %copy-done.9, f32[128,4]{1,0:T(8,128)} %copy.21.refs_1_, f32[128,2048]{1,0:T(8,128)} %shard_map.172.refs_2_, bf16[1536,512]{1,0:T(8,128)(2,1)} %bitcast.32, bf16[192,192]{1,0:T(8,128)(2,1)} %constant.33.clone.place_ref.refs_4_), custom_call_target="tpu_custom_call" | custom-call | tf_op jit(solution)/shard_map/pallas_call | solution.py:328
  (64 shorter events, 17.0 us)
Async XLA Ops:
  7.2 224.1 %copy-start = (bf16[128,2048]{1,0:T(8,128)(2,1)S(1)}, bf16[128,2048]{1,0:T(8,128)(2,1)}, u32[]{:S(2)}) copy-start(bf16[128,2048]{1,0:T(8,128)(2,1)} %param.29) | copy-start | bytes 1572868
  8.0 55.3 %copy-start.9 = (s32[128,4]{1,0:T(8,128)}, s32[128,4]{1,0:T(8,128)S(1)}, u32[]{:S(2)}) copy-start(s32[128,4]{1,0:T(8,128)S(1)} %copy.22.refs_0_) | copy-start | bytes 6148
  63.3 148.8 %all-to-all-start.2 = ((bf16[64,24,512]{2,1,0:T(8,128)(2,1)}), bf16[64,24,512]{2,1,0:T(8,128)(2,1)}, u32[]{:S(2)}, u32[]{:S(2)}) async-start(bf16[64,24,512]{2,1,0:T(8,128)(2,1)} %bitcast.12), calls=%async_computation.3 | async-start | bytes 3145728 | tf_op jit(solution)/shard_map/all_to_all | solution.py:282
  71.8 6.9 %copy-start.1 = (bf16[2,2048,256]{2,1,0:T(8,128)(2,1)S(1)}, bf16[2,2048,256]{2,1,0:T(8,128)(2,1)}, u32[]{:S(2)}) copy-start(bf16[2,2048,256]{2,1,0:T(8,128)(2,1)} %ga_ref.7) | copy-start | bytes 6291460
  71.8 157.0 %all-gather.2.cloned.1.call-start = ((), (), s32[]{:S(2)}) async-start(), calls=%async_computation.5 | async-start | bytes 2621440 | tf_op jit(solution)/shard_map/all_gather | solution.py:316
  71.9 132.3 %collective-permute-start.5 = (bf16[2,256,2048]{2,1,0:T(8,128)(2,1)}, bf16[2,256,2048]{2,1,0:T(8,128)(2,1)}, u32[]{:S(2)}, u32[]{:S(2)}) collective-permute-start(bf16[2,256,2048]{2,1,0:T(8,128)(2,1)} %d0_ref.3), channel_id=1, source_target_pairs={{0,1},{1,0},{2,3},{3,2},{4,5},{5,4},{6,7},{7,6},{8,9},{9,8},{10,11... | collective-permute-start | bytes 6291464 | tf_op jit(solution)/shard_map/ppermute | solution.py:260
  76.6 37.1 %collective-permute-start.6 = (bf16[256,2048]{1,0:T(8,128)(2,1)}, bf16[256,2048]{1,0:T(8,128)(2,1)}, u32[]{:S(2)}, u32[]{:S(2)}) collective-permute-start(bf16[256,2048]{1,0:T(8,128)(2,1)} %get-tuple-element.9), channel_id=1, source_target_pairs={{1,2},{2,1},{3,0},{0,3},{5,6},{6,5},{7,4},{4,7},{9,10},{10,9},{11,... | collective-permute-start | bytes 3145736 | tf_op jit(solution)/shard_map/ppermute | solution.py:260
  78.8 1.8 copy-start.5
  78.8 2.9 copy-start.2
  79.9 80.1 %collective-permute-start.1 = (bf16[2048,256]{1,0:T(8,128)(2,1)S(1)}, bf16[2048,256]{1,0:T(8,128)(2,1)S(1)}, u32[]{:S(2)}, u32[]{:S(2)}) collective-permute-start(bf16[2048,256]{1,0:T(8,128)(2,1)S(1)} %get-tuple-element.13), channel_id=1, source_target_pairs={{0,1},{1,0},{2,3},{3,2},{4,5},{5,4},{6,7},{7,6},{8,9},{9,8},{10,11... | collective-permute-start | bytes 3145736 | tf_op jit(solution)/shard_map/ppermute | solution.py:260
  80.6 101.9 %collective-permute-start.3 = (bf16[1536,512]{1,0:T(8,128)(2,1)S(1)}, bf16[1536,512]{1,0:T(8,128)(2,1)}, u32[]{:S(2)}, u32[]{:S(2)}) collective-permute-start(bf16[1536,512]{1,0:T(8,128)(2,1)S(1)} %bitcast.35), channel_id=1, source_target_pairs={{1,2},{2,1},{3,0},{0,3},{5,6},{6,5},{7,4},{4,7},{9,10},{10,9},{11,... | collective-permute-start | bytes 4718600 | tf_op jit(solution)/shard_map/ppermute | solution.py:260
  82.9 99.6 %collective-permute-start.2 = (bf16[2048,256]{1,0:T(8,128)(2,1)S(1)}, bf16[2048,256]{1,0:T(8,128)(2,1)S(1)}, u32[]{:S(2)}, u32[]{:S(2)}) collective-permute-start(bf16[2048,256]{1,0:T(8,128)(2,1)S(1)} %get-tuple-element.11), channel_id=1, source_target_pairs={{0,1},{1,0},{2,3},{3,2},{4,5},{5,4},{6,7},{7,6},{8,9},{9,8},{10,11... | collective-permute-start | bytes 3145736 | tf_op jit(solution)/shard_map/ppermute | solution.py:260
  113.8 90.4 %collective-permute-start.7 = (bf16[256,2048]{1,0:T(8,128)(2,1)}, bf16[256,2048]{1,0:T(8,128)(2,1)}, u32[]{:S(2)}, u32[]{:S(2)}) collective-permute-start(bf16[256,2048]{1,0:T(8,128)(2,1)} %collective-permute-done.6.d2_ref), channel_id=1, source_target_pairs={{0,1},{1,0},{2,3},{3,2},{4,5},{5,4},{6,7},{7,6},{8,9},{9,8},{10,11... | collective-permute-start | bytes 3145736 | tf_op jit(solution)/shard_map/ppermute | solution.py:260
  160.0 22.5 %copy-start.6 = (bf16[2048,256]{1,0:T(8,128)(2,1)}, bf16[2048,256]{1,0:T(8,128)(2,1)S(1)}, u32[]{:S(2)}) copy-start(bf16[2048,256]{1,0:T(8,128)(2,1)S(1)} %collective-permute-done.1.gb_ref) | copy-start | bytes 3145732
  182.5 1.0 copy-start.7
  190.4 13.9 %collective-permute-start.4 = (bf16[384,512]{1,0:T(8,128)(2,1)}, bf16[384,512]{1,0:T(8,128)(2,1)S(1)}, u32[]{:S(2)}, u32[]{:S(2)}) collective-permute-start(bf16[384,512]{1,0:T(8,128)(2,1)} %shard_map.170), channel_id=1, source_target_pairs={{1,2},{2,1},{3,0},{0,3},{5,6},{6,5},{7,4},{4,7},{9,10},{10,9},{11,... | collective-permute-start | bytes 1179656 | tf_op jit(solution)/shard_map/ppermute | solution.py:260
  212.1 16.7 %copy-start.10 = (bf16[2048,128]{1,0:T(8,128)(2,1)S(1)}, bf16[2048,128]{1,0:T(8,128)(2,1)}, u32[]{:S(2)}) copy-start(bf16[2048,128]{1,0:T(8,128)(2,1)} %param.27) | copy-start | bytes 1572868
  212.1 130.4 %all-to-all-start.1 = ((bf16[64,24,512]{2,1,0:T(8,128)(2,1)}), bf16[64,24,512]{2,1,0:T(8,128)(2,1)}, u32[]{:S(2)}, u32[]{:S(2)}) async-start(bf16[64,24,512]{2,1,0:T(8,128)(2,1)} %bitcast.33), calls=%async_computation.2 | async-start | bytes 3145728 | tf_op jit(solution)/shard_map/all_to_all | solution.py:282
  222.7 176.5 %reduce-scatter.2.cloned.1.call-start = ((), (), s32[]{:S(2)}) async-start(), calls=%async_computation.6 | async-start | bytes 2621440 | tf_op jit(solution)/shard_map/reduce_scatter | solution.py:321
  222.7 28.4 %collective-permute-start.8 = (bf16[2048,256]{1,0:T(8,128)(2,1)}, bf16[2048,256]{1,0:T(8,128)(2,1)}, u32[]{:S(2)}, u32[]{:S(2)}) collective-permute-start(bf16[2048,256]{1,0:T(8,128)(2,1)} %get-tuple-element.12), channel_id=1, source_target_pairs={{1,2},{2,1},{3,0},{0,3},{5,6},{6,5},{7,4},{4,7},{9,10},{10,9},{11,... | collective-permute-start | bytes 3145736 | tf_op jit(solution)/shard_map/ppermute | solution.py:260
  225.6 64.1 %collective-permute-start.9 = (bf16[2048,256]{1,0:T(8,128)(2,1)}, bf16[2048,256]{1,0:T(8,128)(2,1)}, u32[]{:S(2)}, u32[]{:S(2)}) collective-permute-start(bf16[2048,256]{1,0:T(8,128)(2,1)} %get-tuple-element.10), channel_id=1, source_target_pairs={{1,2},{2,1},{3,0},{0,3},{5,6},{6,5},{7,4},{4,7},{9,10},{10,9},{11,... | collective-permute-start | bytes 3145736 | tf_op jit(solution)/shard_map/ppermute | solution.py:260
  226.1 86.1 %collective-permute-start.12 = (bf16[256,2048]{1,0:T(8,128)(2,1)}, bf16[256,2048]{1,0:T(8,128)(2,1)}, u32[]{:S(2)}, u32[]{:S(2)}) collective-permute-start(bf16[256,2048]{1,0:T(8,128)(2,1)} %get-tuple-element.8), channel_id=1, source_target_pairs={{1,2},{2,1},{3,0},{0,3},{5,6},{6,5},{7,4},{4,7},{9,10},{10,9},{11,... | collective-permute-start | bytes 3145736 | tf_op jit(solution)/shard_map/ppermute | solution.py:260
  228.8 60.9 %collective-permute-start.10 = (bf16[1536,512]{1,0:T(8,128)(2,1)}, bf16[1536,512]{1,0:T(8,128)(2,1)}, u32[]{:S(2)}, u32[]{:S(2)}) collective-permute-start(bf16[1536,512]{1,0:T(8,128)(2,1)} %bitcast.13.x_ref), channel_id=1, source_target_pairs={{0,1},{1,0},{2,3},{3,2},{4,5},{5,4},{6,7},{7,6},{8,9},{9,8},{10,11... | collective-permute-start | bytes 4718600 | tf_op jit(solution)/shard_map/ppermute | solution.py:260
  228.8 2.5 copy-start.3
  237.3 96.4 %collective-permute-start.13 = (bf16[256,2048]{1,0:T(8,128)(2,1)S(1)}, bf16[256,2048]{1,0:T(8,128)(2,1)S(1)}, u32[]{:S(2)}, u32[]{:S(2)}) collective-permute-start(bf16[256,2048]{1,0:T(8,128)(2,1)S(1)} %slice_bitcast_fusion), channel_id=1, source_target_pairs={{1,2},{2,1},{3,0},{0,3},{5,6},{6,5},{7,4},{4,7},{9,10},{10,9},{11,... | collective-permute-start | bytes 3145736 | tf_op jit(solution)/shard_map/ppermute | solution.py:260
  296.6 37.1 %collective-permute-start.11 = (bf16[384,512]{1,0:T(8,128)(2,1)}, bf16[384,512]{1,0:T(8,128)(2,1)S(1)}, u32[]{:S(2)}, u32[]{:S(2)}) collective-permute-start(bf16[384,512]{1,0:T(8,128)(2,1)} %shard_map.174), channel_id=1, source_target_pairs={{0,1},{1,0},{2,3},{3,2},{4,5},{5,4},{6,7},{7,6},{8,9},{9,8},{10,11... | collective-permute-start | bytes 1179656 | tf_op jit(solution)/shard_map/ppermute | solution.py:260
  333.7 1.0 copy-start.8
  342.5 11.4 %copy-start.14 = (f32[2048]{0:T(1024)S(1)}, f32[2048]{0:T(1024)}, u32[]{:S(2)}) copy-start(f32[2048]{0:T(1024)} %param.17) | copy-start | bytes 24580
  342.5 14.8 %copy-start.15 = (f32[128,4]{0,1:T(4,128)S(1)}, f32[128,4]{0,1:T(4,128)}, u32[]{:S(2)}) copy-start(f32[128,4]{0,1:T(4,128)} %param.23) | copy-start | bytes 6148
  342.5 62.3 %all-to-all-start.3 = ((bf16[64,24,512]{2,1,0:T(8,128)(2,1)}), bf16[64,24,512]{2,1,0:T(8,128)(2,1)S(1)}, u32[]{:S(2)}, u32[]{:S(2)}) async-start(bf16[64,24,512]{2,1,0:T(8,128)(2,1)} %bitcast.36), calls=%async_computation.4 | async-start | bytes 3145728 | tf_op jit(solution)/shard_map/all_to_all | solution.py:282
  354.8 39.1 %collective-permute-start = (bf16[16,2048]{1,0:T(8,128)(2,1)S(1)}, bf16[16,2048]{1,0:T(8,128)(2,1)S(1)}, u32[]{:S(2)}, u32[]{:S(2)}) collective-permute-start(bf16[16,2048]{1,0:T(8,128)(2,1)S(1)} %fusion.8), channel_id=1, source_target_pairs={{0,1},{1,2},{2,3},{3,4},{4,5},{5,6},{6,7},{7,8},{8,9},{9,10},{10,1... | collective-permute-start | bytes 196616 | tf_op jit(solution)/shard_map/ppermute | solution.py:211
  404.8 1.2 copy-start.4
  (3 other events, 2.1 us)
Sparse Core Ops, SparseCore 0:
  78.9 49.7 all-gather.1
  236.1 49.5 reduce-scatter.1

commit v2 on v1

v2 whole, which is shorter than its diff:
```python
import functools

import jax
import jax.numpy as jnp
import numpy as np
from jax import lax
from jax.experimental import pallas as pl
from jax.experimental.pallas import tpu as pltpu
from jax.sharding import PartitionSpec as P


WINDOWS = (2, 4, 8, 16)
RMS_EPS = 1e-06
ROUTED_SCALE = 2.5
CAP = 6
COLS = 4
PACK = CAP * COLS
BLOCK = 8
SEND_BLOCK = 16
PAIR_A = ((0, 1), (1, 0), (2, 3), (3, 2))
PAIR_B = ((1, 2), (2, 1), (3, 0), (0, 3))


f32 = jnp.float32
bf16 = jnp.bfloat16


def dot32(a, b):
    return jnp.dot(a, b, preferred_element_type=f32)


def call(body, out, scratch=(), count=0, smem=(), hbm=()):
    def spec(i):
        if i in hbm:
            return pl.BlockSpec(memory_space=pltpu.HBM)
        return pl.BlockSpec(memory_space=pltpu.SMEM if i in smem else pltpu.VMEM)

    return pl.pallas_call(
        body, out_shape=out, in_specs=[spec(i) for i in range(count)], scratch_shapes=list(scratch)
    )


def unpack_matrix():
    rows = BLOCK * PACK
    per = BLOCK * CAP
    place = np.zeros((rows, rows), np.float32)
    for i in range(rows):
        q, rest = divmod(i, per)
        j, s = divmod(rest, CAP)
        place[i, j * PACK + q * CAP + s] = 1.0
    return place


def norm_send_body(at_ref, x_ref, gain_ref, ids_ref, h_ref, m_ref, rank_ref, hcat_ref):
    h_ref[...] = rms_norm(x_ref[...], gain_ref[...])
    send_rows(0, at_ref, h_ref, ids_ref, m_ref, rank_ref, hcat_ref)


def send_body(at_ref, h_ref, ids_ref, m_ref, rank_ref, hcat_ref):
    send_rows(1, at_ref, h_ref, ids_ref, m_ref, rank_ref, hcat_ref)


def send_rows(e, at_ref, h_ref, ids_ref, m_ref, rank_ref, hcat_ref):
    toks, width = h_ref.shape
    part = width // COLS
    for q in range(COLS):
        hcat_ref[q * toks : (q + 1) * toks, :] = h_ref[:, q * part : (q + 1) * part]
    peers = rank_ref.shape[0]
    ids = ids_ref[:, pl.ds(pl.multiple_of(at_ref[0] * toks, toks), toks)]
    expert = 2 * lax.broadcasted_iota(jnp.int32, (peers, toks), 0) + e
    named = jnp.zeros((peers, toks), f32)
    for k in range(ids.shape[0]):
        named = named + (ids[k : k + 1, :] == expert).astype(f32)
    before = (
        lax.broadcasted_iota(jnp.int32, (toks, toks), 0)
        < lax.broadcasted_iota(jnp.int32, (toks, toks), 1)
    ).astype(f32).astype(bf16)
    rank = jnp.where(named > 0, dot32(named.astype(bf16), before), -1.0)
    for q in range(COLS):
        rank_ref[:, q * toks : (q + 1) * toks] = rank

    def block(b, _):
        ranks = rank_ref[pl.ds(pl.multiple_of(b * SEND_BLOCK, SEND_BLOCK), SEND_BLOCK), :]
        shape = (SEND_BLOCK, PACK, COLS * toks)
        r = lax.broadcasted_iota(jnp.int32, shape, 1)
        col = lax.broadcasted_iota(jnp.int32, shape, 2)
        q = sum((r >= CAP * i).astype(jnp.int32) for i in range(1, COLS))
        want = jnp.where(
            (col >= q * toks) & (col < (q + 1) * toks), (r - CAP * q).astype(f32), -2.0
        )
        pick = (jnp.broadcast_to(ranks[:, None, :], shape) == want).astype(f32)
        pick = pick.reshape(SEND_BLOCK * PACK, COLS * toks).astype(bf16)
        rows = SEND_BLOCK * PACK
        m_ref[pl.ds(pl.multiple_of(b * rows, rows), rows), :] = dot32(
            pick, hcat_ref[...]
        ).astype(bf16)
        return 0

    lax.fori_loop(0, peers // SEND_BLOCK, block, 0)


def fetch(sources, targets, sems):
    copies = [
        pltpu.make_async_copy(src, dst, sems.at[i])
        for i, (src, dst) in enumerate(zip(sources, targets))
    ]
    for copy in copies:
        copy.start()
    return copies


def plane(ref, e):
    return ref.at[e] if len(ref.shape) == 3 else ref


def unpack_into(x_ref, place_ref, rows_ref):
    rows = BLOCK * PACK
    per = BLOCK * CAP
    part = x_ref.shape[1]

    def block(b, _):
        got = dot32(
            place_ref[...], x_ref[pl.ds(pl.multiple_of(b * rows, rows), rows), :]
        ).astype(bf16)
        for q in range(COLS):
            rows_ref[
                pl.ds(pl.multiple_of(b * per, per), per), q * part : (q + 1) * part
            ] = got[q * per : (q + 1) * per, :]
        return 0

    lax.fori_loop(0, x_ref.shape[0] // rows, block, 0, unroll=4)


def hidden_body(e, x_ref, place_ref, ga, ua, ub, *refs):
    *gb, hid_ref, rows_ref, held_ref, sems = refs
    w = held_ref.shape[1] // 4
    tall = held_ref.shape[0] // len(gb)
    targets = [held_ref.at[:, i * w : (i + 1) * w] for i in (0, 2, 3)]
    targets += [held_ref.at[i * tall : (i + 1) * tall, w : 2 * w] for i in range(len(gb))]
    copies = fetch([plane(ref, e) for ref in (ga, ua, ub, *gb)], targets, sems)
    unpack_into(x_ref, place_ref, rows_ref)
    for copy in copies:
        copy.wait()
    both = dot32(rows_ref[...], held_ref[...])
    gate = both[:, : 2 * w]
    hid_ref[...] = (gate / (1.0 + jnp.exp(-gate)) * both[:, 2 * w :]).astype(bf16)


def down_body(
    e, mine_ref, theirs_ref, d0, d1, d2, d3, place_ref, out_ref, y_ref, held_ref, hid_ref, sems
):
    w = mine_ref.shape[1] // 2
    cols = held_ref.shape[1] // 2
    sides = [slice(c * cols, (c + 1) * cols) for c in range(2)]
    copies = [
        fetch(
            [plane(ref, e).at[:, side] for ref in (d0, d1, d2, d3)],
            [held_ref.at[i * w : (i + 1) * w, side] for i in range(4)],
            sems.at[pl.ds(4 * c, 4)],
        )
        for c, side in enumerate(sides)
    ]
    hid_ref[:, : 2 * w] = mine_ref[...]
    hid_ref[:, 2 * w :] = theirs_ref[...]
    for side, group in zip(sides, copies):
        for copy in group:
            copy.wait()
        y_ref[:, side] = dot32(hid_ref[...], held_ref[:, side]).astype(bf16)
    rows = BLOCK * PACK
    per = BLOCK * CAP
    part = out_ref.shape[1]

    def block(b, _):
        at = pl.ds(pl.multiple_of(b * per, per), per)
        stack = jnp.concatenate(
            [y_ref[at, q * part : (q + 1) * part] for q in range(COLS)], axis=0
        )
        out_ref[pl.ds(pl.multiple_of(b * rows, rows), rows), :] = dot32(
            place_ref[...], stack
        ).astype(bf16)
        return 0

    lax.fori_loop(0, y_ref.shape[0] // per, block, 0, unroll=4)


def route_matrix(e, ids, score, peers):
    toks = ids.shape[0]
    total = peers * CAP
    weight = score / jnp.sum(score, axis=1, keepdims=True) * ROUTED_SCALE
    expert = 2 * lax.broadcasted_iota(jnp.int32, (toks, peers), 1) + e
    named = jnp.zeros((toks, peers), f32)
    scaled = jnp.zeros((toks, peers), f32)
    for k in range(ids.shape[1]):
        hit = ids[:, k : k + 1] == expert
        named = named + hit.astype(f32)
        scaled = scaled + jnp.where(hit, weight[:, k : k + 1], 0.0)
    before = (
        lax.broadcasted_iota(jnp.int32, (toks, toks), 1)
        < lax.broadcasted_iota(jnp.int32, (toks, toks), 0)
    ).astype(f32).astype(bf16)
    rank = jnp.where(named > 0, dot32(before, named.astype(bf16)), -1.0).astype(bf16)
    at = lax.broadcasted_iota(jnp.int32, (peers, total), 1) - CAP * lax.broadcasted_iota(
        jnp.int32, (peers, total), 0
    )
    mine = (at >= 0) & (at < CAP)
    spread = mine.astype(f32).astype(bf16)
    slot = jnp.sum(jnp.where(mine, at, 0).astype(f32), axis=0, keepdims=True)
    here = dot32(rank, spread) == slot
    high = scaled.astype(bf16)
    low = (scaled - high.astype(f32)).astype(bf16)
    return [jnp.where(here, dot32(piece, spread), 0.0).astype(bf16) for piece in (high, low)]


def first_body(
    at_ref, ids_ref, score_ref, base_ref, r_ref, place_ref, acc_ref, route_ref, rows_ref
):
    unpack_into(r_ref, place_ref, rows_ref)
    score = score_ref[...]
    toks = score.shape[0]
    ids = ids_ref[pl.ds(pl.multiple_of(at_ref[0] * toks, toks), toks), :]
    peers = rows_ref.shape[0] // CAP
    acc = base_ref[...]
    for piece in route_matrix(0, ids, score, peers):
        acc = acc + dot32(piece, rows_ref[...])
    acc_ref[...] = acc
    route_ref[:toks, :], route_ref[toks:, :] = route_matrix(1, ids, score, peers)


def last_body(acc_ref, more_ref, route_ref, r_ref, place_ref, out_ref, rows_ref):
    unpack_into(r_ref, place_ref, rows_ref)
    toks = acc_ref.shape[0]
    both = dot32(route_ref[...], rows_ref[...])
    acc = acc_ref[...] + more_ref[...].astype(f32) + both[:toks] + both[toks:]
    out_ref[...] = acc.astype(bf16)


def shared_body(own_ref, other_ref, ga, ua, da, gb, ub, db, own_out_ref, other_out_ref):
    for h_ref, out_ref in ((other_ref, other_out_ref), (own_ref, own_out_ref)):
        h = h_ref[...]
        total = None
        for g_ref, u_ref, d_ref in ((ga, ua, da), (gb, ub, db)):
            gate = dot32(h, g_ref[...])
            up = dot32(h, u_ref[...])
            hidden = (gate / (1.0 + jnp.exp(-gate)) * up).astype(bf16)
            piece = dot32(hidden, d_ref[...])
            total = piece if total is None else total + piece
        out_ref[...] = total.astype(out_ref.dtype)


def rms_norm(values, gain_row):
    upcast = values.astype(f32)
    scaled = upcast * lax.rsqrt(jnp.mean(upcast * upcast, axis=-1, keepdims=True) + RMS_EPS)
    return (scaled * gain_row).astype(bf16)


def mixer_body(at_ref, x_ref, gain_ref, halo_ref, pool_ref, scale_ref, out_ref, rows_ref):
    lead = halo_ref.shape[0]
    rows, width = x_ref.shape
    group = width // len(WINDOWS)
    rows_ref[:lead, :] = halo_ref[...]
    rows_ref[lead:, :] = rms_norm(x_ref[...], gain_ref[...])
    ahead = lax.broadcasted_iota(jnp.int32, (rows, lead + rows), 0) + lead
    back = ahead - lax.broadcasted_iota(jnp.int32, (rows, lead + rows), 1)
    taken = at_ref[0] + 1 + lax.broadcasted_iota(jnp.int32, (rows, 1), 0)
    for g, span in enumerate(WINDOWS):
        cols = slice(g * group, (g + 1) * group)
        band = ((back >= 0) & (back < span)).astype(f32).astype(bf16)
        pooled = dot32(band, rows_ref[:, cols]) / jnp.minimum(taken, span).astype(f32)
        difference = (pooled - rows_ref[lead:, cols].astype(f32)).astype(bf16)
        out_ref[:, cols] = (dot32(difference, pool_ref[g]) * scale_ref[:, cols]).astype(bf16)


def tail_before(mix_input, mix_gain):
    lead = max(WINDOWS)
    length = lax.axis_size(("ep", "tp"))
    return lax.ppermute(
        rms_norm(mix_input[mix_input.shape[0] - lead :], mix_gain),
        ("ep", "tp"),
        [(i, i + 1) for i in range(length - 1)],
    )


def mixer(mix_input, mix_gain, before, pool_weight, pool_scale):
    rows, width = mix_input.shape
    lead = before.shape[0]
    offset = (lax.axis_index(("ep", "tp")) * rows).astype(jnp.int32)
    return call(
        mixer_body,
        jax.ShapeDtypeStruct((rows, width), bf16),
        (pltpu.VMEM((lead + rows, width), bf16),),
        smem=(0,),
        count=6,
    )(offset[None], mix_input, mix_gain[None, :], before, pool_weight, pool_scale[None, :])


def layer(
    mix_input,
    mix_gain,
    pool_weight,
    pool_scale,
    moe_input,
    moe_gain,
    expert_ids,
    route_score,
    expert_gate,
    expert_up,
    expert_down,
    shared_gate,
    shared_up,
    shared_down,
):
    toks, width = moe_input.shape
    peers = lax.axis_size("ep")
    quarter = lax.axis_index("tp")
    part = width // COLS
    packed = peers * PACK
    slots = peers * CAP
    place = jnp.asarray(unpack_matrix(), bf16)
    place_back = jnp.asarray(unpack_matrix().T, bf16)
    at = quarter.astype(jnp.int32)[None]

    pairs = (PAIR_A, PAIR_B)

    def swap(value, pairs):
        return lax.ppermute(value, "tp", pairs)

    def cut(value, at):
        return value[at]

    pairs = (PAIR_A, PAIR_B)
    half = width // 2
    gates = [
        [swap(expert_gate[0], PAIR_A)],
        [swap(expert_gate[1, i * half :][:half], PAIR_B) for i in range(2)],
    ]
    ups = [swap(cut(expert_up, e), pairs[e]) for e in range(2)]
    down_a = swap(expert_down, PAIR_A)
    down_b = swap(expert_down, PAIR_B)
    across = [swap(cut(down_b, 0), PAIR_A), swap(cut(down_a, 1), PAIR_B)]

    ranking = (pltpu.VMEM((peers, COLS * toks), f32), pltpu.VMEM((COLS * toks, part), bf16))
    message = jax.ShapeDtypeStruct((packed, part), bf16)
    h, send = call(
        norm_send_body,
        (jax.ShapeDtypeStruct((toks, width), bf16), message),
        ranking,
        count=4,
        smem=(0,),
    )(at, moe_input, moe_gain[None, :], expert_ids.T)
    sends = (
        send,
        call(send_body, message, ranking, count=3, smem=(0,))(at, h, expert_ids.T),
    )

    def over_ep(value):
        value = value.reshape(peers, PACK, part)
        return lax.all_to_all(value, "ep", 0, 0, tiled=True).reshape(packed, part)

    ff = expert_gate.shape[2]
    unpacking = (pltpu.VMEM((slots, width), bf16),)

    def hidden_half(rows, e):
        return call(
            functools.partial(hidden_body, e),
            jax.ShapeDtypeStruct((slots, 2 * ff), bf16),
            (
                *unpacking,
                pltpu.VMEM((width, 4 * ff), bf16),
                pltpu.SemaphoreType.DMA((5,)),
            ),
            count=5 + len(gates[e]),
            hbm=tuple(range(2, 5 + len(gates[e]))),
        )(rows, place, expert_gate, expert_up, ups[e], *gates[e])

    back = []
    for e in range(2):
        own = over_ep(sends[e])
        other = swap(own, pairs[1 - e])
        mine = hidden_half(own, e)
        theirs = hidden_half(other, e)
        theirs = swap(theirs, pairs[1 - e])
        weights = (expert_down, down_a, down_b, across[0])
        if e == 1:
            weights = (expert_down, down_b, down_a, across[1])
        back.append(
            call(
                functools.partial(down_body, e),
                jax.ShapeDtypeStruct((packed, part), bf16),
                (
                    pltpu.VMEM((slots, width), bf16),
                    pltpu.VMEM((4 * ff, width), bf16),
                    pltpu.VMEM((slots, 4 * ff), bf16),
                    pltpu.SemaphoreType.DMA((8,)),
                ),
                count=7,
                hbm=(2, 3, 4, 5),
            )(mine, theirs, *weights, place_back)
        )

    near = [swap(w, PAIR_A) for w in (shared_gate, shared_up, shared_down)]
    visitors = swap(h, PAIR_B)
    shared_own, shared_other = call(
        shared_body,
        (
            jax.ShapeDtypeStruct((toks, width), f32),
            jax.ShapeDtypeStruct((toks, width), bf16),
        ),
        count=8,
    )(h, visitors, shared_gate, shared_up, shared_down, *near)
    shared_more = swap(shared_other, PAIR_B)

    halo = tail_before(mix_input, mix_gain)
    mix_output = mixer(mix_input, mix_gain, halo, pool_weight, pool_scale)

    returned = over_ep(back[0])
    acc, route = call(
        first_body,
        (jax.ShapeDtypeStruct((toks, width), f32), jax.ShapeDtypeStruct((2 * toks, slots), bf16)),
        unpacking,
        count=6,
        smem=(0,),
    )(at, expert_ids, route_score, shared_own, returned, place)
    returned = over_ep(back[1])
    moe_output = call(
        last_body, jax.ShapeDtypeStruct((toks, width), bf16), unpacking, count=5
    )(acc, shared_more, route, returned, place)
    return (mix_output, moe_output)


def solution(mesh):
    return jax.shard_map(
        layer,
        mesh=mesh,
        in_specs=(
            P(("ep", "tp"), None),
            P(),
            P(),
            P(),
            P(("ep", "tp"), None),
            P(),
            P("ep", None),
            P(("ep", "tp"), None),
            P("ep", None, "tp"),
            P("ep", None, "tp"),
            P("ep", "tp", None),
            P(None, "tp"),
            P(None, "tp"),
            P("tp", None),
        ),
        out_specs=(P(("ep", "tp"), None), P(("ep", "tp"), None)),
        check_vma=False,
    )
```

time: 419 us -> 382 us (0.912); the launches traced: 418 us -> 374 us
  blocking collectives: 47.3 us -> 0 us
  starting transfers between devices: 47.9 us -> 68.7 us
  between operations: 14.2 us -> 0.92 us
  matrix products: 7.13 us -> 0 us
    all_to_all x1 -> x0, blocking collectives: 47.3 us -> none  [over_ep(): return lax.all_to_all(value, 'ep', 0, 0, tiled=True).reshape(packed, part)]
    all_to_all x3 -> x4, waiting for transfers between devices: 0.01 us -> 30.3 us  [over_ep(): return lax.all_to_all(value, 'ep', 0, 0, tiled=True).reshape(packed, part)]
    ppermute x1, waiting for transfers between devices: 35.9 us -> 6.1 us  [tail_before(): lax.ppermute(rms_norm(mix_input[mix_input.shape[0] - lead:], mix_gain), (...]
    ppermute x13 -> x18, starting transfers between devices: 15.9 us -> 26.7 us  [swap(): return lax.ppermute(value, 'tp', pairs)]
    all_to_all x3 -> x4, starting transfers between devices: 29.5 us -> 39.8 us  [over_ep(): return lax.all_to_all(value, 'ep', 0, 0, tiled=True).reshape(packed, part)]
    dot_general x2 -> x0, matrix products: 7.13 us -> none  [dot32(): return jnp.dot(a, b, preferred_element_type=f32)]
    unnamed x34 -> x48, local copies, waits for them, and re-layouts: 6.22 us -> 8.99 us
    ppermute x13 -> x18, waiting for transfers between devices: 185 us -> 187 us  [swap(): return lax.ppermute(value, 'tp', pairs)]
  transfers between devices with their start and end apart: 19 -> 23, of which waited for: 9 -> 12; matrix products, arithmetic and copies ran while one was open for 4% -> 3% of each run, Pallas kernels for 12% -> 15%
where the time goes in v2:
time: 382 us; the launch traced here: 374 us
  waiting for transfers between devices  224 us (59%)
  starting transfers between devices  68.7 us (18%)
  Pallas kernels  64.4 us (17%)
  local copies, waits for them, and re-layouts  14.9 us (4%)
    ppermute x18, waiting for transfers between devices, swap(): return lax.ppermute(value, 'tp', pairs)  187 us
    all_to_all x4, starting transfers between devices, over_ep(): return lax.all_to_all(value, 'ep', 0, 0, tiled=True).reshape(packed, part)  39.8 us
    all_to_all x4, waiting for transfers between devices, over_ep(): return lax.all_to_all(value, 'ep', 0, 0, tiled=True).reshape(packed, part)  30.3 us
    ppermute x18, starting transfers between devices, swap(): return lax.ppermute(value, 'tp', pairs)  26.7 us
    pallas_call x4, Pallas kernels, hidden_half(): call(functools.partial(hidden_body, e), jax.ShapeDtypeStruct((slots, 2 *...  24.6 us
    pallas_call x2, Pallas kernels, layer(): call(functools.partial(down_body, e), jax.ShapeDtypeStruct((packed, part)...  13.2 us
    unnamed x48, local copies, waits for them, and re-layouts  8.99 us
  transfers between devices with their start and end apart: 23, of which 12 were waited for; matrix products, arithmetic and copies ran while one was open for 3% of the time, Pallas kernels for 15%

profile of v2, /device:TPU:160, one launch (start us, length us, event | category | flops | bytes accessed | tf_op | source)
XLA Modules:
  0.0 374.4 jit_solution(3330615412489015067)
XLA Ops:
  0.6 3.9 %shard_map.168 = (bf16[128,2048]{1,0:T(8,128)(2,1)}, bf16[1536,512]{1,0:T(8,128)(2,1)}) custom-call(s32[1]{0:T(128)} %bitcast.3.at_ref, bf16[128,2048]{1,0:T(8,128)(2,1)} %x_ref.3, f32[1,2048]{1,0:T(1,128)} %bitcast.36, s32[4,512]{1,0:T(4,128)} %bitcast.33), custom_call_target="tpu_custom_call" | custom-call | tf_op jit(solution)/shard_map/pallas_call | solution.py:343
  4.6 10.3 %all-to-all-start = ((bf16[64,24,512]{2,1,0:T(8,128)(2,1)}), bf16[64,24,512]{2,1,0:T(8,128)(2,1)}, u32[]{:S(2)}, u32[]{:S(2)}) async-start(bf16[64,24,512]{2,1,0:T(8,128)(2,1)} %bitcast.32), calls=%async_computation | async-start | bytes 3145728 | tf_op jit(solution)/shard_map/all_to_all | solution.py:357
  14.8 2.8 collective-permute-start.10
  17.7 3.9 %shard_map.174 = bf16[1536,512]{1,0:T(8,128)(2,1)} custom-call(s32[1]{0:T(128)} %bitcast.3.at_ref, bf16[128,2048]{1,0:T(8,128)(2,1)} %get-tuple-element.8.own_ref.h_ref, s32[4,512]{1,0:T(4,128)} %bitcast.34), custom_call_target="tpu_custom_call" | custom-call | tf_op jit(solution)/shard_map/pallas_call | solution.py:352
  21.6 30.3 %all-to-all-done = bf16[64,24,512]{2,1,0:T(8,128)(2,1)} async-done(((bf16[64,24,512]{2,1,0:T(8,128)(2,1)}), bf16[64,24,512]{2,1,0:T(8,128)(2,1)}, u32[]{:S(2)}, u32[]{:S(2)}) %all-to-all-start) | async-done | bytes 1572896 | tf_op jit(solution)/shard_map/all_to_all | solution.py:357
  51.9 8.5 %all-to-all-start.2 = ((bf16[64,24,512]{2,1,0:T(8,128)(2,1)}), bf16[64,24,512]{2,1,0:T(8,128)(2,1)}, u32[]{:S(2)}, u32[]{:S(2)}) async-start(bf16[64,24,512]{2,1,0:T(8,128)(2,1)} %bitcast.30), calls=%async_computation.2 | async-start | bytes 3145728 | tf_op jit(solution)/shard_map/all_to_all | solution.py:357
  63.6 2.8 collective-permute-start.7
  66.8 2.3 slice_bitcast_fusion.1
  70.9 60.8 %collective-permute-done.5.ub = bf16[2048,256]{1,0:T(8,128)(2,1)S(1)} collective-permute-done((bf16[2048,256]{1,0:T(8,128)(2,1)S(1)}, bf16[2048,256]{1,0:T(8,128)(2,1)S(1)}, u32[]{:S(2)}, u32[]{:S(2)}) %collective-permute-start.5) | collective-permute-done | bytes 1048608 | tf_op jit(solution)/shard_map/ppermute | solution.py:325
  131.7 22.5 %collective-permute-done.6.refs_0_ = bf16[2048,256]{1,0:T(8,128)(2,1)S(1)} collective-permute-done((bf16[2048,256]{1,0:T(8,128)(2,1)S(1)}, bf16[2048,256]{1,0:T(8,128)(2,1)S(1)}, u32[]{:S(2)}, u32[]{:S(2)}) %collective-permute-start.6) | collective-permute-done | bytes 1048608 | tf_op jit(solution)/shard_map/ppermute | solution.py:325
  155.1 6.2 %shard_map.171 = bf16[384,512]{1,0:T(8,128)(2,1)} custom-call(bf16[1536,512]{1,0:T(8,128)(2,1)} %collective-permute-done.7.x_ref, bf16[192,192]{1,0:T(8,128)(2,1)} %constant.24.clone.place_ref, bf16[2,2048,256]{2,1,0:T(8,128)(2,1)} %ga.9, bf16[2,2048,256]{2,1,0:T(8,128)(2,1)} %ua.9, bf16[2048,256]{1,0:T(8,128)(2,1)} %copy-done.5, bf16[2048,256]{1,0:T(8,128)(2,1)} %copy-done.6), custom_call_target="tpu_custom_call" | custom-call | tf_op jit(solution)/shard_map/pallas_call | solution.py:363
  161.3 3.0 collective-permute-start.8
  164.3 6.2 %shard_map.170.mine_ref = bf16[384,512]{1,0:T(8,128)(2,1)} custom-call(bf16[1536,512]{1,0:T(8,128)(2,1)} %bitcast.7.x_ref, bf16[192,192]{1,0:T(8,128)(2,1)} %constant.24.clone.place_ref, bf16[2,2048,256]{2,1,0:T(8,128)(2,1)} %ga.9, bf16[2,2048,256]{2,1,0:T(8,128)(2,1)} %ua.9, bf16[2048,256]{1,0:T(8,128)(2,1)} %copy-done.5, bf16[2048,256]{1,0:T(8,128)(2,1)} %copy-done.6), custom_call_target="tpu_custom_call" | custom-call | tf_op jit(solution)/shard_map/pallas_call | solution.py:363
  170.5 5.3 %collective-permute-done.11.d3 = bf16[256,2048]{1,0:T(8,128)(2,1)S(1)} collective-permute-done((bf16[256,2048]{1,0:T(8,128)(2,1)}, bf16[256,2048]{1,0:T(8,128)(2,1)S(1)}, u32[]{:S(2)}, u32[]{:S(2)}) %collective-permute-start.11) | collective-permute-done | bytes 1048608 | tf_op jit(solution)/shard_map/ppermute | solution.py:325
  177.5 6.7 %shard_map.172 = bf16[1536,512]{1,0:T(8,128)(2,1)} custom-call(bf16[384,512]{1,0:T(8,128)(2,1)} %shard_map.170.mine_ref, bf16[384,512]{1,0:T(8,128)(2,1)} %copy-done.18, bf16[2,256,2048]{2,1,0:T(8,128)(2,1)} %d0.3, bf16[2,256,2048]{2,1,0:T(8,128)(2,1)} %collective-permute-done.9.d1.d2, bf16[2,256,2048]{2,1,0:T(8,128)(2,1)} %collective-permute-done.10.d2.d1, ...), custom_call_target="tpu_custom_call" | custom-call | tf_op jit(solution)/shard_map/pallas_call | solution.py:386
  184.2 10.6 %all-to-all-start.1 = ((bf16[64,24,512]{2,1,0:T(8,128)(2,1)}), bf16[64,24,512]{2,1,0:T(8,128)(2,1)}, u32[]{:S(2)}, u32[]{:S(2)}) async-start(bf16[64,24,512]{2,1,0:T(8,128)(2,1)} %bitcast.29), calls=%async_computation.1 | async-start | bytes 3145728 | tf_op jit(solution)/shard_map/all_to_all | solution.py:357
  198.5 2.4 slice_bitcast_fusion
  205.4 52.2 %collective-permute-done.14.refs_0_ = bf16[1024,256]{1,0:T(8,128)(2,1)S(1)} collective-permute-done((bf16[1024,256]{1,0:T(8,128)(2,1)S(1)}, bf16[1024,256]{1,0:T(8,128)(2,1)S(1)}, u32[]{:S(2)}, u32[]{:S(2)}) %collective-permute-start.14) | collective-permute-done | bytes 524320 | tf_op jit(solution)/shard_map/ppermute | solution.py:325
  257.6 10.1 %collective-permute-done.15.refs_1_ = bf16[1024,256]{1,0:T(8,128)(2,1)S(1)} collective-permute-done((bf16[1024,256]{1,0:T(8,128)(2,1)S(1)}, bf16[1024,256]{1,0:T(8,128)(2,1)S(1)}, u32[]{:S(2)}, u32[]{:S(2)}) %collective-permute-start.15) | collective-permute-done | bytes 524320 | tf_op jit(solution)/shard_map/ppermute | solution.py:325
  268.8 6.1 %shard_map.176 = bf16[384,512]{1,0:T(8,128)(2,1)} custom-call(bf16[1536,512]{1,0:T(8,128)(2,1)} %collective-permute-done.16.x_ref, bf16[192,192]{1,0:T(8,128)(2,1)} %constant.24.clone.place_ref, bf16[2,2048,256]{2,1,0:T(8,128)(2,1)} %ga.9, bf16[2,2048,256]{2,1,0:T(8,128)(2,1)} %ua.9, bf16[2048,256]{1,0:T(8,128)(2,1)} %copy-done.4, ...), custom_call_target="tpu_custom_call" | custom-call | tf_op jit(solution)/shard_map/pallas_call | solution.py:363
  275.3 6.2 %shard_map.175.mine_ref = bf16[384,512]{1,0:T(8,128)(2,1)} custom-call(bf16[1536,512]{1,0:T(8,128)(2,1)} %bitcast.14.x_ref, bf16[192,192]{1,0:T(8,128)(2,1)} %constant.24.clone.place_ref, bf16[2,2048,256]{2,1,0:T(8,128)(2,1)} %ga.9, bf16[2,2048,256]{2,1,0:T(8,128)(2,1)} %ua.9, bf16[2048,256]{1,0:T(8,128)(2,1)} %copy-done.4, bf16[1024,256]{1,0:T(8,128)(2,1)} %copy-done.7, ...), custom_call_target="tpu_custom_call" | custom-call | tf_op jit(solution)/shard_map/pallas_call | solution.py:363
  281.5 4.0 %collective-permute-done.17.theirs_ref = bf16[384,512]{1,0:T(8,128)(2,1)S(1)} collective-permute-done((bf16[384,512]{1,0:T(8,128)(2,1)}, bf16[384,512]{1,0:T(8,128)(2,1)S(1)}, u32[]{:S(2)}, u32[]{:S(2)}) %collective-permute-start.17) | collective-permute-done | bytes 393248 | tf_op jit(solution)/shard_map/ppermute | solution.py:325
  286.2 6.6 %shard_map.177 = bf16[1536,512]{1,0:T(8,128)(2,1)} custom-call(bf16[384,512]{1,0:T(8,128)(2,1)} %shard_map.175.mine_ref, bf16[384,512]{1,0:T(8,128)(2,1)} %copy-done.17, bf16[2,256,2048]{2,1,0:T(8,128)(2,1)} %d0.3, bf16[2,256,2048]{2,1,0:T(8,128)(2,1)} %collective-permute-done.10.d2.d1, bf16[2,256,2048]{2,1,0:T(8,128)(2,1)} %collective-permute-done.9.d1.d2, ...), custom_call_target="tpu_custom_call" | custom-call | tf_op jit(solution)/shard_map/pallas_call | solution.py:386
  292.8 10.4 %all-to-all-start.3 = ((bf16[64,24,512]{2,1,0:T(8,128)(2,1)}), bf16[64,24,512]{2,1,0:T(8,128)(2,1)S(1)}, u32[]{:S(2)}, u32[]{:S(2)}) async-start(bf16[64,24,512]{2,1,0:T(8,128)(2,1)} %bitcast.28), calls=%async_computation.3 | async-start | bytes 3145728 | tf_op jit(solution)/shard_map/all_to_all | solution.py:357
  308.6 9.9 %collective-permute-done.1.other_ref = bf16[128,2048]{1,0:T(8,128)(2,1)S(1)} collective-permute-done((bf16[128,2048]{1,0:T(8,128)(2,1)S(1)}, bf16[128,2048]{1,0:T(8,128)(2,1)S(1)}, u32[]{:S(2)}, u32[]{:S(2)}) %collective-permute-start.1) | collective-permute-done | bytes 524320 | tf_op jit(solution)/shard_map/ppermute | solution.py:325
  320.3 11.2 %collective-permute-done.3.ub = bf16[2048,128]{1,0:T(8,128)(2,1)S(1)} collective-permute-done((bf16[2048,128]{1,0:T(8,128)(2,1)S(1)}, bf16[2048,128]{1,0:T(8,128)(2,1)S(1)}, u32[]{:S(2)}, u32[]{:S(2)}) %collective-permute-start.3) | collective-permute-done | bytes 524320 | tf_op jit(solution)/shard_map/ppermute | solution.py:325
  332.3 9.4 %collective-permute-done.4.db = bf16[128,2048]{1,0:T(8,128)(2,1)} collective-permute-done((bf16[128,2048]{1,0:T(8,128)(2,1)}, bf16[128,2048]{1,0:T(8,128)(2,1)}, u32[]{:S(2)}, u32[]{:S(2)}) %collective-permute-start.4) | collective-permute-done | bytes 524320 | tf_op jit(solution)/shard_map/ppermute | solution.py:325
  341.7 5.2 %shard_map.169 = (f32[128,2048]{1,0:T(8,128)}, bf16[128,2048]{1,0:T(8,128)(2,1)}) custom-call(bf16[128,2048]{1,0:T(8,128)(2,1)} %get-tuple-element.8.own_ref.h_ref, bf16[128,2048]{1,0:T(8,128)(2,1)} %copy-done.14, bf16[2048,128]{1,0:T(8,128)(2,1)} %ga.5, bf16[2048,128]{1,0:T(8,128)(2,1)} %ua.5, bf16[128,2048]{1,0:T(8,128)(2,1)} %da.1, ...), custom_call_target="tpu_custom_call" | custom-call | tf_op jit(solution)/shard_map/pallas_call | solution.py:402
  352.8 6.1 %collective-permute-done.halo_ref = bf16[16,2048]{1,0:T(8,128)(2,1)S(1)} collective-permute-done((bf16[16,2048]{1,0:T(8,128)(2,1)S(1)}, bf16[16,2048]{1,0:T(8,128)(2,1)S(1)}, u32[]{:S(2)}, u32[]{:S(2)}) %collective-permute-start) | collective-permute-done | bytes 65568 | tf_op jit(solution)/shard_map/ppermute | solution.py:276
  359.5 4.7 %shard_map.167 = bf16[256,2048]{1,0:T(8,128)(2,1)} custom-call(s32[1]{0:T(128)} %bitcast.at_ref, bf16[256,2048]{1,0:T(8,128)(2,1)} %x_ref.2, f32[1,2048]{1,0:T(1,128)} %bitcast.35, bf16[16,2048]{1,0:T(8,128)(2,1)} %copy-done.20, bf16[4,512,512]{2,1,0:T(8,128)(2,1)} %pool_ref.1, f32[1,2048]{1,0:T(1,128)} %bitcast.37), custom_call_target="tpu_custom_call" | custom-call | tf_op jit(solution)/shard_map/pallas_call | solution.py:287
  364.2 4.7 %shard_map.173 = (f32[128,2048]{1,0:T(8,128)}, bf16[256,384]{1,0:T(8,128)(2,1)}) custom-call(s32[1]{0:T(128)} %bitcast.3.at_ref, s32[512,4]{1,0:T(8,128)} %copy.18.ids_ref, f32[128,4]{1,0:T(8,128)} %copy.19.score_ref, f32[128,2048]{1,0:T(8,128)} %get-tuple-element.9.base_ref, bf16[1536,512]{1,0:T(8,128)(2,1)} %bitcast.12.r_ref, ...), custom_call_target="tpu_custom_call" | custom-call | tf_op jit(solution)/shard_map/pallas_call | solution.py:416
  370.2 4.1 %shard_map.178 = bf16[128,2048]{1,0:T(8,128)(2,1)} custom-call(f32[128,2048]{1,0:T(8,128)} %get-tuple-element.11.acc_ref, bf16[128,2048]{1,0:T(8,128)(2,1)} %copy-done.11, bf16[256,384]{1,0:T(8,128)(2,1)} %get-tuple-element.13.route_ref, bf16[1536,512]{1,0:T(8,128)(2,1)} %bitcast.31, bf16[192,192]{1,0:T(8,128)(2,1)} %constant.24.clone.place_ref), custom_call_target="tpu_custom_call" | custom-call | tf_op jit(solution)/shard_map/pallas_call | solution.py:424
  (82 shorter events, 34.2 us)
Async XLA Ops:
  4.6 47.3 %all-to-all-start = ((bf16[64,24,512]{2,1,0:T(8,128)(2,1)}), bf16[64,24,512]{2,1,0:T(8,128)(2,1)}, u32[]{:S(2)}, u32[]{:S(2)}) async-start(bf16[64,24,512]{2,1,0:T(8,128)(2,1)} %bitcast.32), calls=%async_computation | async-start | bytes 3145728 | tf_op jit(solution)/shard_map/all_to_all | solution.py:357
  14.8 51.9 %collective-permute-start.10 = (bf16[2,256,2048]{2,1,0:T(8,128)(2,1)}, bf16[2,256,2048]{2,1,0:T(8,128)(2,1)}, u32[]{:S(2)}, u32[]{:S(2)}) collective-permute-start(bf16[2,256,2048]{2,1,0:T(8,128)(2,1)} %d0.3), channel_id=1, source_target_pairs={{1,2},{2,1},{3,0},{0,3},{5,6},{6,5},{7,4},{4,7},{9,10},{10,9},{11,... | collective-permute-start | bytes 6291464 | tf_op jit(solution)/shard_map/ppermute | solution.py:325
  21.6 40.4 %copy-start.2 = (bf16[2,2048,256]{2,1,0:T(8,128)(2,1)S(1)}, bf16[2,2048,256]{2,1,0:T(8,128)(2,1)}, u32[]{:S(2)}) copy-start(bf16[2,2048,256]{2,1,0:T(8,128)(2,1)} %ua.9) | copy-start | bytes 6291460
  51.9 132.3 %all-to-all-start.2 = ((bf16[64,24,512]{2,1,0:T(8,128)(2,1)}), bf16[64,24,512]{2,1,0:T(8,128)(2,1)}, u32[]{:S(2)}, u32[]{:S(2)}) async-start(bf16[64,24,512]{2,1,0:T(8,128)(2,1)} %bitcast.30), calls=%async_computation.2 | async-start | bytes 3145728 | tf_op jit(solution)/shard_map/all_to_all | solution.py:357
  60.4 110.1 %collective-permute-start.9 = (bf16[2,256,2048]{2,1,0:T(8,128)(2,1)}, bf16[2,256,2048]{2,1,0:T(8,128)(2,1)}, u32[]{:S(2)}, u32[]{:S(2)}) collective-permute-start(bf16[2,256,2048]{2,1,0:T(8,128)(2,1)} %d0.3), channel_id=1, source_target_pairs={{0,1},{1,0},{2,3},{3,2},{4,5},{5,4},{6,7},{7,6},{8,9},{9,8},{10,11... | collective-permute-start | bytes 6291464 | tf_op jit(solution)/shard_map/ppermute | solution.py:325
  63.1 68.6 %collective-permute-start.5 = (bf16[2048,256]{1,0:T(8,128)(2,1)S(1)}, bf16[2048,256]{1,0:T(8,128)(2,1)S(1)}, u32[]{:S(2)}, u32[]{:S(2)}) collective-permute-start(bf16[2048,256]{1,0:T(8,128)(2,1)S(1)} %get-tuple-element.17), channel_id=1, source_target_pairs={{0,1},{1,0},{2,3},{3,2},{4,5},{5,4},{6,7},{7,6},{8,9},{9,8},{10,11... | collective-permute-start | bytes 3145736 | tf_op jit(solution)/shard_map/ppermute | solution.py:325
  63.6 90.5 %collective-permute-start.7 = (bf16[1536,512]{1,0:T(8,128)(2,1)}, bf16[1536,512]{1,0:T(8,128)(2,1)}, u32[]{:S(2)}, u32[]{:S(2)}) collective-permute-start(bf16[1536,512]{1,0:T(8,128)(2,1)} %bitcast.7.x_ref), channel_id=1, source_target_pairs={{1,2},{2,1},{3,0},{0,3},{5,6},{6,5},{7,4},{4,7},{9,10},{10,9},{11,... | collective-permute-start | bytes 4718600 | tf_op jit(solution)/shard_map/ppermute | solution.py:325
  66.4 87.7 %collective-permute-start.6 = (bf16[2048,256]{1,0:T(8,128)(2,1)S(1)}, bf16[2048,256]{1,0:T(8,128)(2,1)S(1)}, u32[]{:S(2)}, u32[]{:S(2)}) collective-permute-start(bf16[2048,256]{1,0:T(8,128)(2,1)S(1)} %slice_bitcast_fusion.3), channel_id=1, source_target_pairs={{0,1},{1,0},{2,3},{3,2},{4,5},{5,4},{6,7},{7,6},{8,9},{9,8},{10,11... | collective-permute-start | bytes 3145736 | tf_op jit(solution)/shard_map/ppermute | solution.py:325
  69.1 106.7 %collective-permute-start.11 = (bf16[256,2048]{1,0:T(8,128)(2,1)}, bf16[256,2048]{1,0:T(8,128)(2,1)S(1)}, u32[]{:S(2)}, u32[]{:S(2)}) collective-permute-start(bf16[256,2048]{1,0:T(8,128)(2,1)} %slice_bitcast_fusion.1), channel_id=1, source_target_pairs={{0,1},{1,0},{2,3},{3,2},{4,5},{5,4},{6,7},{7,6},{8,9},{9,8},{10,11... | collective-permute-start | bytes 3145736 | tf_op jit(solution)/shard_map/ppermute | solution.py:325
  131.7 22.5 %copy-start.5 = (bf16[2048,256]{1,0:T(8,128)(2,1)}, bf16[2048,256]{1,0:T(8,128)(2,1)S(1)}, u32[]{:S(2)}) copy-start(bf16[2048,256]{1,0:T(8,128)(2,1)S(1)} %collective-permute-done.5.ub) | copy-start | bytes 3145732
  161.3 14.5 %collective-permute-start.8 = (bf16[384,512]{1,0:T(8,128)(2,1)}, bf16[384,512]{1,0:T(8,128)(2,1)S(1)}, u32[]{:S(2)}, u32[]{:S(2)}) collective-permute-start(bf16[384,512]{1,0:T(8,128)(2,1)} %shard_map.171), channel_id=1, source_target_pairs={{1,2},{2,1},{3,0},{0,3},{5,6},{6,5},{7,4},{4,7},{9,10},{10,9},{11,... | collective-permute-start | bytes 1179656 | tf_op jit(solution)/shard_map/ppermute | solution.py:325
  184.2 17.8 %copy-start.1 = (bf16[2,2048,256]{2,1,0:T(8,128)(2,1)S(1)}, bf16[2,2048,256]{2,1,0:T(8,128)(2,1)}, u32[]{:S(2)}) copy-start(bf16[2,2048,256]{2,1,0:T(8,128)(2,1)} %ga.9) | copy-start | bytes 6291460
  184.2 108.6 %all-to-all-start.1 = ((bf16[64,24,512]{2,1,0:T(8,128)(2,1)}), bf16[64,24,512]{2,1,0:T(8,128)(2,1)}, u32[]{:S(2)}, u32[]{:S(2)}) async-start(bf16[64,24,512]{2,1,0:T(8,128)(2,1)} %bitcast.29), calls=%async_computation.1 | async-start | bytes 3145728 | tf_op jit(solution)/shard_map/all_to_all | solution.py:357
  194.8 72.9 %collective-permute-start.16 = (bf16[1536,512]{1,0:T(8,128)(2,1)}, bf16[1536,512]{1,0:T(8,128)(2,1)}, u32[]{:S(2)}, u32[]{:S(2)}) collective-permute-start(bf16[1536,512]{1,0:T(8,128)(2,1)} %bitcast.14.x_ref), channel_id=1, source_target_pairs={{0,1},{1,0},{2,3},{3,2},{4,5},{5,4},{6,7},{7,6},{8,9},{9,8},{10,11... | collective-permute-start | bytes 4718600 | tf_op jit(solution)/shard_map/ppermute | solution.py:325
  196.4 71.3 %collective-permute-start.13 = (bf16[2048,256]{1,0:T(8,128)(2,1)}, bf16[2048,256]{1,0:T(8,128)(2,1)S(1)}, u32[]{:S(2)}, u32[]{:S(2)}) collective-permute-start(bf16[2048,256]{1,0:T(8,128)(2,1)} %get-tuple-element.16), channel_id=1, source_target_pairs={{1,2},{2,1},{3,0},{0,3},{5,6},{6,5},{7,4},{4,7},{9,10},{10,9},{11,... | collective-permute-start | bytes 3145736 | tf_op jit(solution)/shard_map/ppermute | solution.py:325
  200.8 80.6 %collective-permute-start.18 = (bf16[256,2048]{1,0:T(8,128)(2,1)}, bf16[256,2048]{1,0:T(8,128)(2,1)}, u32[]{:S(2)}, u32[]{:S(2)}) collective-permute-start(bf16[256,2048]{1,0:T(8,128)(2,1)} %slice_bitcast_fusion), channel_id=1, source_target_pairs={{1,2},{2,1},{3,0},{0,3},{5,6},{6,5},{7,4},{4,7},{9,10},{10,9},{11,... | collective-permute-start | bytes 3145736 | tf_op jit(solution)/shard_map/ppermute | solution.py:325
  202.1 55.5 %collective-permute-start.14 = (bf16[1024,256]{1,0:T(8,128)(2,1)S(1)}, bf16[1024,256]{1,0:T(8,128)(2,1)S(1)}, u32[]{:S(2)}, u32[]{:S(2)}) collective-permute-start(bf16[1024,256]{1,0:T(8,128)(2,1)S(1)} %get-tuple-element.15), channel_id=1, source_target_pairs={{1,2},{2,1},{3,0},{0,3},{5,6},{6,5},{7,4},{4,7},{9,10},{10,9},{11,... | collective-permute-start | bytes 1572872 | tf_op jit(solution)/shard_map/ppermute | solution.py:325
  204.2 63.4 %collective-permute-start.15 = (bf16[1024,256]{1,0:T(8,128)(2,1)S(1)}, bf16[1024,256]{1,0:T(8,128)(2,1)S(1)}, u32[]{:S(2)}, u32[]{:S(2)}) collective-permute-start(bf16[1024,256]{1,0:T(8,128)(2,1)S(1)} %get-tuple-element.14), channel_id=1, source_target_pairs={{1,2},{2,1},{3,0},{0,3},{5,6},{6,5},{7,4},{4,7},{9,10},{10,9},{11,... | collective-permute-start | bytes 1572872 | tf_op jit(solution)/shard_map/ppermute | solution.py:325
  274.9 10.5 %collective-permute-start.17 = (bf16[384,512]{1,0:T(8,128)(2,1)}, bf16[384,512]{1,0:T(8,128)(2,1)S(1)}, u32[]{:S(2)}, u32[]{:S(2)}) collective-permute-start(bf16[384,512]{1,0:T(8,128)(2,1)} %shard_map.176), channel_id=1, source_target_pairs={{0,1},{1,0},{2,3},{3,2},{4,5},{5,4},{6,7},{7,6},{8,9},{9,8},{10,11... | collective-permute-start | bytes 1179656 | tf_op jit(solution)/shard_map/ppermute | solution.py:325
  292.8 12.7 %copy-start.12 = (bf16[2048,128]{1,0:T(8,128)(2,1)S(1)}, bf16[2048,128]{1,0:T(8,128)(2,1)}, u32[]{:S(2)}) copy-start(bf16[2048,128]{1,0:T(8,128)(2,1)} %ga.5) | copy-start | bytes 1572868
  292.8 12.7 %copy-start.13 = (bf16[2048,128]{1,0:T(8,128)(2,1)S(1)}, bf16[2048,128]{1,0:T(8,128)(2,1)}, u32[]{:S(2)}) copy-start(bf16[2048,128]{1,0:T(8,128)(2,1)} %ua.5) | copy-start | bytes 1572868
  292.8 76.1 %all-to-all-start.3 = ((bf16[64,24,512]{2,1,0:T(8,128)(2,1)}), bf16[64,24,512]{2,1,0:T(8,128)(2,1)S(1)}, u32[]{:S(2)}, u32[]{:S(2)}) async-start(bf16[64,24,512]{2,1,0:T(8,128)(2,1)} %bitcast.28), calls=%async_computation.3 | async-start | bytes 3145728 | tf_op jit(solution)/shard_map/all_to_all | solution.py:357
  303.3 15.2 %collective-permute-start.1 = (bf16[128,2048]{1,0:T(8,128)(2,1)S(1)}, bf16[128,2048]{1,0:T(8,128)(2,1)S(1)}, u32[]{:S(2)}, u32[]{:S(2)}) collective-permute-start(bf16[128,2048]{1,0:T(8,128)(2,1)S(1)} %copy-done.9), channel_id=1, source_target_pairs={{1,2},{2,1},{3,0},{0,3},{5,6},{6,5},{7,4},{4,7},{9,10},{10,9},{11,... | collective-permute-start | bytes 1572872 | tf_op jit(solution)/shard_map/ppermute | solution.py:325
  305.5 14.8 %collective-permute-start.2 = (bf16[2048,128]{1,0:T(8,128)(2,1)S(1)}, bf16[2048,128]{1,0:T(8,128)(2,1)S(1)}, u32[]{:S(2)}, u32[]{:S(2)}) collective-permute-start(bf16[2048,128]{1,0:T(8,128)(2,1)S(1)} %copy-done.12), channel_id=1, source_target_pairs={{0,1},{1,0},{2,3},{3,2},{4,5},{5,4},{6,7},{7,6},{8,9},{9,8},{10,11... | collective-permute-start | bytes 1572872 | tf_op jit(solution)/shard_map/ppermute | solution.py:325
  305.5 26.0 %collective-permute-start.3 = (bf16[2048,128]{1,0:T(8,128)(2,1)S(1)}, bf16[2048,128]{1,0:T(8,128)(2,1)S(1)}, u32[]{:S(2)}, u32[]{:S(2)}) collective-permute-start(bf16[2048,128]{1,0:T(8,128)(2,1)S(1)} %copy-done.13), channel_id=1, source_target_pairs={{0,1},{1,0},{2,3},{3,2},{4,5},{5,4},{6,7},{7,6},{8,9},{9,8},{10,11... | collective-permute-start | bytes 1572872 | tf_op jit(solution)/shard_map/ppermute | solution.py:325
  307.5 34.2 %collective-permute-start.4 = (bf16[128,2048]{1,0:T(8,128)(2,1)}, bf16[128,2048]{1,0:T(8,128)(2,1)}, u32[]{:S(2)}, u32[]{:S(2)}) collective-permute-start(bf16[128,2048]{1,0:T(8,128)(2,1)} %da.1), channel_id=1, source_target_pairs={{0,1},{1,0},{2,3},{3,2},{4,5},{5,4},{6,7},{7,6},{8,9},{9,8},{10,11... | collective-permute-start | bytes 1572872 | tf_op jit(solution)/shard_map/ppermute | solution.py:325
  308.6 39.5 %copy-start.21 = (f32[2048]{0:T(1024)S(1)}, f32[2048]{0:T(1024)}, u32[]{:S(2)}) copy-start(f32[2048]{0:T(1024)} %param.17) | copy-start | bytes 24580
  308.6 42.6 %copy-start.19 = (s32[512,4]{0,1:T(4,128)S(1)}, s32[512,4]{0,1:T(4,128)}, u32[]{:S(2)}) copy-start(s32[512,4]{0,1:T(4,128)} %param.22) | copy-start | bytes 24580
  308.6 43.4 %copy-start.22 = (f32[128,4]{0,1:T(4,128)S(1)}, f32[128,4]{0,1:T(4,128)}, u32[]{:S(2)}) copy-start(f32[128,4]{0,1:T(4,128)} %param.23) | copy-start | bytes 6148
  318.5 13.0 %copy-start.14 = (bf16[128,2048]{1,0:T(8,128)(2,1)}, bf16[128,2048]{1,0:T(8,128)(2,1)S(1)}, u32[]{:S(2)}) copy-start(bf16[128,2048]{1,0:T(8,128)(2,1)S(1)} %collective-permute-done.1.other_ref) | copy-start | bytes 1572868
  346.9 22.0 %collective-permute-start.12 = (bf16[128,2048]{1,0:T(8,128)(2,1)}, bf16[128,2048]{1,0:T(8,128)(2,1)S(1)}, u32[]{:S(2)}, u32[]{:S(2)}) collective-permute-start(bf16[128,2048]{1,0:T(8,128)(2,1)} %get-tuple-element.12), channel_id=1, source_target_pairs={{1,2},{2,1},{3,0},{0,3},{5,6},{6,5},{7,4},{4,7},{9,10},{10,9},{11,... | collective-permute-start | bytes 1572872 | tf_op jit(solution)/shard_map/ppermute | solution.py:325
  348.9 9.9 %collective-permute-start = (bf16[16,2048]{1,0:T(8,128)(2,1)S(1)}, bf16[16,2048]{1,0:T(8,128)(2,1)S(1)}, u32[]{:S(2)}, u32[]{:S(2)}) collective-permute-start(bf16[16,2048]{1,0:T(8,128)(2,1)S(1)} %fusion.2), channel_id=1, source_target_pairs={{0,1},{1,2},{2,3},{3,4},{4,5},{5,6},{6,7},{7,8},{8,9},{9,10},{10,1... | collective-permute-start | bytes 196616 | tf_op jit(solution)/shard_map/ppermute | solution.py:276
  (14 other events, 46.8 us)

commit v3 on v2

--- a/solution.py
+++ b/solution.py
@@ -17,6 +17,7 @@
 PACK = CAP * COLS
 BLOCK = 8
 SEND_BLOCK = 16
+LATE_ROWS = 11
 PAIR_A = ((0, 1), (1, 0), (2, 3), (3, 2))
 PAIR_B = ((1, 2), (2, 1), (3, 0), (0, 3))
 
@@ -135,28 +136,30 @@
     *gb, hid_ref, rows_ref, held_ref, sems = refs
     w = held_ref.shape[1] // 4
     tall = held_ref.shape[0] // len(gb)
-    targets = [held_ref.at[:, i * w : (i + 1) * w] for i in (0, 2, 3)]
-    targets += [held_ref.at[i * tall : (i + 1) * tall, w : 2 * w] for i in range(len(gb))]
+    targets = [held_ref.at[:, i * w : (i + 1) * w] for i in (0, 1, 3)]
+    targets += [held_ref.at[i * tall : (i + 1) * tall, 2 * w : 3 * w] for i in range(len(gb))]
     copies = fetch([plane(ref, e) for ref in (ga, ua, ub, *gb)], targets, sems)
     unpack_into(x_ref, place_ref, rows_ref)
-    for copy in copies:
-        copy.wait()
-    both = dot32(rows_ref[...], held_ref[...])
-    gate = both[:, : 2 * w]
-    hid_ref[...] = (gate / (1.0 + jnp.exp(-gate)) * both[:, 2 * w :]).astype(bf16)
-
-
-def down_body(
-    e, mine_ref, theirs_ref, d0, d1, d2, d3, place_ref, out_ref, y_ref, held_ref, hid_ref, sems
-):
+    for i, group in enumerate((copies[:2], copies[2:])):
+        for copy in group:
+            copy.wait()
+        gate = dot32(rows_ref[...], held_ref[:, 2 * i * w : (2 * i + 1) * w])
+        up = dot32(rows_ref[...], held_ref[:, (2 * i + 1) * w : (2 * i + 2) * w])
+        hid_ref[:, i * w : (i + 1) * w] = (gate / (1.0 + jnp.exp(-gate)) * up).astype(bf16)
+
+
+def down_body(e, mine_ref, theirs_ref, place_ref, *refs):
+    *pieces, out_ref, y_ref, held_ref, hid_ref, sems = refs
     w = mine_ref.shape[1] // 2
     cols = held_ref.shape[1] // 2
     sides = [slice(c * cols, (c + 1) * cols) for c in range(2)]
+    pieces = [plane(ref, e) for ref in pieces]
+    ends = [sum(ref.shape[0] for ref in pieces[:i]) for i in range(len(pieces) + 1)]
     copies = [
         fetch(
-            [plane(ref, e).at[:, side] for ref in (d0, d1, d2, d3)],
-            [held_ref.at[i * w : (i + 1) * w, side] for i in range(4)],
-            sems.at[pl.ds(4 * c, 4)],
+            [ref.at[:, side] for ref in pieces],
+            [held_ref.at[i:j, side] for i, j in zip(ends, ends[1:])],
+            sems.at[pl.ds(len(pieces) * c, len(pieces))],
         )
         for c, side in enumerate(sides)
     ]
@@ -334,10 +337,9 @@
         [swap(expert_gate[1, i * half :][:half], PAIR_B) for i in range(2)],
     ]
     ups = [swap(cut(expert_up, e), pairs[e]) for e in range(2)]
-    down_a = swap(expert_down, PAIR_A)
     down_b = swap(expert_down, PAIR_B)
-    across = [swap(cut(down_b, 0), PAIR_A), swap(cut(down_a, 1), PAIR_B)]
-
+    down_a = [swap(cut(expert_down, 0), PAIR_A)]
+    cross = [swap(cut(down_b, 0), PAIR_A)]
     ranking = (pltpu.VMEM((peers, COLS * toks), f32), pltpu.VMEM((COLS * toks, part), bf16))
     message = jax.ShapeDtypeStruct((packed, part), bf16)
     h, send = call(
@@ -347,6 +349,12 @@
         count=4,
         smem=(0,),
     )(at, moe_input, moe_gain[None, :], expert_ids.T)
+    late_down, _ = lax.optimization_barrier((expert_down, h))
+    early = LATE_ROWS * expert_down.shape[1] // 16
+    for span in (slice(0, early), slice(early, None)):
+        down_a.append(swap(cut(late_down, (1, span)), PAIR_A))
+        cross.append(swap(down_a[-1], PAIR_B))
+
     sends = (
         send,
         call(send_body, message, ranking, count=3, smem=(0,))(at, h, expert_ids.T),
@@ -379,9 +387,9 @@
         mine = hidden_half(own, e)
         theirs = hidden_half(other, e)
         theirs = swap(theirs, pairs[1 - e])
-        weights = (expert_down, down_a, down_b, across[0])
+        weights = (expert_down, down_a[0], down_b, cross[0])
         if e == 1:
-            weights = (expert_down, down_b, down_a, across[1])
+            weights = (expert_down, down_b, *down_a[1:], *cross[1:])
         back.append(
             call(
                 functools.partial(down_body, e),
@@ -390,11 +398,11 @@
                     pltpu.VMEM((slots, width), bf16),
                     pltpu.VMEM((4 * ff, width), bf16),
                     pltpu.VMEM((slots, 4 * ff), bf16),
-                    pltpu.SemaphoreType.DMA((8,)),
+                    pltpu.SemaphoreType.DMA((2 * len(weights),)),
                 ),
-                count=7,
-                hbm=(2, 3, 4, 5),
-            )(mine, theirs, *weights, place_back)
+                count=3 + len(weights),
+                hbm=tuple(range(3, 3 + len(weights))),
+            )(mine, theirs, place_back, *weights)
         )
 
     near = [swap(w, PAIR_A) for w in (shared_gate, shared_up, shared_down)]

time: 382 us -> 348 us (0.911)
  the two profiles are of different devices: /device:TPU:160 before, /device:TPU:1 now
where the time goes in v3:
time: 348 us; the launch traced here: 347 us
  waiting for transfers between devices  192 us (55%)
  starting transfers between devices  72.4 us (21%)
  Pallas kernels  62.8 us (18%)
  local copies, waits for them, and re-layouts  17.1 us (5%)
    ppermute x21, waiting for transfers between devices, swap(): return lax.ppermute(value, 'tp', pairs)  148 us
    all_to_all x4, starting transfers between devices, over_ep(): return lax.all_to_all(value, 'ep', 0, 0, tiled=True).reshape(packed, part)  43.9 us
    all_to_all x4, waiting for transfers between devices, over_ep(): return lax.all_to_all(value, 'ep', 0, 0, tiled=True).reshape(packed, part)  32.6 us
    ppermute x21, starting transfers between devices, swap(): return lax.ppermute(value, 'tp', pairs)  26.3 us
    pallas_call x4, Pallas kernels, hidden_half(): call(functools.partial(hidden_body, e), jax.ShapeDtypeStruct((slots, 2 *...  23.1 us
    pallas_call x2, Pallas kernels, layer(): call(functools.partial(down_body, e), jax.ShapeDtypeStruct((packed, part)...  13.2 us
    ppermute x1, waiting for transfers between devices, tail_before(): lax.ppermute(rms_norm(mix_input[mix_input.shape[0] - lead:], mix_gain), (...  11.4 us
    unnamed x54, local copies, waits for them, and re-layouts  9.08 us
  transfers between devices with their start and end apart: 26, of which 12 were waited for; matrix products, arithmetic and copies ran while one was open for 3% of the time, Pallas kernels for 16%

profile of v3, /device:TPU:1, one launch (start us, length us, event | category | flops | bytes accessed | tf_op | source)
XLA Modules:
  0.0 347.3 jit_solution(15841142130855793671)
XLA Ops:
  0.6 4.0 %shard_map.168 = (bf16[128,2048]{1,0:T(8,128)(2,1)}, bf16[1536,512]{1,0:T(8,128)(2,1)}) custom-call(s32[1]{0:T(128)} %bitcast.3.at_ref, bf16[128,2048]{1,0:T(8,128)(2,1)} %x_ref.3, f32[1,2048]{1,0:T(1,128)} %bitcast.40, s32[4,512]{1,0:T(4,128)} %bitcast.37), custom_call_target="tpu_custom_call" | custom-call | tf_op jit(solution)/shard_map/pallas_call | solution.py:345
  4.6 13.3 %all-to-all-start = ((bf16[64,24,512]{2,1,0:T(8,128)(2,1)}), bf16[64,24,512]{2,1,0:T(8,128)(2,1)}, u32[]{:S(2)}, u32[]{:S(2)}) async-start(bf16[64,24,512]{2,1,0:T(8,128)(2,1)} %bitcast.36), calls=%async_computation | async-start | bytes 3145728 | tf_op jit(solution)/shard_map/all_to_all | solution.py:365
  17.9 2.6 collective-permute-start.10
  20.5 3.8 %shard_map.174 = bf16[1536,512]{1,0:T(8,128)(2,1)} custom-call(s32[1]{0:T(128)} %bitcast.3.at_ref, bf16[128,2048]{1,0:T(8,128)(2,1)} %get-tuple-element.9.own_ref.h_ref, s32[4,512]{1,0:T(4,128)} %bitcast.38), custom_call_target="tpu_custom_call" | custom-call | tf_op jit(solution)/shard_map/pallas_call | solution.py:360
  24.3 32.6 %all-to-all-done = bf16[64,24,512]{2,1,0:T(8,128)(2,1)} async-done(((bf16[64,24,512]{2,1,0:T(8,128)(2,1)}), bf16[64,24,512]{2,1,0:T(8,128)(2,1)}, u32[]{:S(2)}, u32[]{:S(2)}) %all-to-all-start) | async-done | bytes 1572896 | tf_op jit(solution)/shard_map/all_to_all | solution.py:365
  56.9 6.5 %all-to-all-start.2 = ((bf16[64,24,512]{2,1,0:T(8,128)(2,1)}), bf16[64,24,512]{2,1,0:T(8,128)(2,1)}, u32[]{:S(2)}, u32[]{:S(2)}) async-start(bf16[64,24,512]{2,1,0:T(8,128)(2,1)} %bitcast.32), calls=%async_computation.2 | async-start | bytes 3145728 | tf_op jit(solution)/shard_map/all_to_all | solution.py:365
  74.8 14.1 %collective-permute-done.5.ub = bf16[2048,256]{1,0:T(8,128)(2,1)S(1)} collective-permute-done((bf16[2048,256]{1,0:T(8,128)(2,1)S(1)}, bf16[2048,256]{1,0:T(8,128)(2,1)S(1)}, u32[]{:S(2)}, u32[]{:S(2)}) %collective-permute-start.5) | collective-permute-done | bytes 1048608 | tf_op jit(solution)/shard_map/ppermute | solution.py:328
  88.9 22.4 %collective-permute-done.6.refs_0_ = bf16[2048,256]{1,0:T(8,128)(2,1)S(1)} collective-permute-done((bf16[2048,256]{1,0:T(8,128)(2,1)S(1)}, bf16[2048,256]{1,0:T(8,128)(2,1)S(1)}, u32[]{:S(2)}, u32[]{:S(2)}) %collective-permute-start.6) | collective-permute-done | bytes 1048608 | tf_op jit(solution)/shard_map/ppermute | solution.py:328
  112.2 5.8 %shard_map.171 = bf16[384,512]{1,0:T(8,128)(2,1)} custom-call(bf16[1536,512]{1,0:T(8,128)(2,1)} %collective-permute-done.7.x_ref, bf16[192,192]{1,0:T(8,128)(2,1)} %constant.24.clone.place_ref, bf16[2,2048,256]{2,1,0:T(8,128)(2,1)} %ga.9, bf16[2,2048,256]{2,1,0:T(8,128)(2,1)} %ua.9, bf16[2048,256]{1,0:T(8,128)(2,1)} %copy-done.5, bf16[2048,256]{1,0:T(8,128)(2,1)} %copy-done.6), custom_call_target="tpu_custom_call" | custom-call | tf_op jit(solution)/shard_map/pallas_call | solution.py:371
  118.0 2.7 collective-permute-start.8
  120.8 5.8 %shard_map.170.mine_ref = bf16[384,512]{1,0:T(8,128)(2,1)} custom-call(bf16[1536,512]{1,0:T(8,128)(2,1)} %bitcast.7.x_ref, bf16[192,192]{1,0:T(8,128)(2,1)} %constant.24.clone.place_ref, bf16[2,2048,256]{2,1,0:T(8,128)(2,1)} %ga.9, bf16[2,2048,256]{2,1,0:T(8,128)(2,1)} %ua.9, bf16[2048,256]{1,0:T(8,128)(2,1)} %copy-done.5, bf16[2048,256]{1,0:T(8,128)(2,1)} %copy-done.6), custom_call_target="tpu_custom_call" | custom-call | tf_op jit(solution)/shard_map/pallas_call | solution.py:371
  126.5 7.2 %collective-permute-done.9.refs_1_ = bf16[256,2048]{1,0:T(8,128)(2,1)S(1)} collective-permute-done((bf16[256,2048]{1,0:T(8,128)(2,1)}, bf16[256,2048]{1,0:T(8,128)(2,1)S(1)}, u32[]{:S(2)}, u32[]{:S(2)}) %collective-permute-start.9) | collective-permute-done | bytes 1048608 | tf_op jit(solution)/shard_map/ppermute | solution.py:328
  133.7 22.6 %collective-permute-done.11.refs_3_ = bf16[256,2048]{1,0:T(8,128)(2,1)} collective-permute-done((bf16[256,2048]{1,0:T(8,128)(2,1)}, bf16[256,2048]{1,0:T(8,128)(2,1)}, u32[]{:S(2)}, u32[]{:S(2)}) %collective-permute-start.11) | collective-permute-done | bytes 1048608 | tf_op jit(solution)/shard_map/ppermute | solution.py:328
  157.1 6.6 %shard_map.172 = bf16[1536,512]{1,0:T(8,128)(2,1)} custom-call(bf16[384,512]{1,0:T(8,128)(2,1)} %shard_map.170.mine_ref, bf16[384,512]{1,0:T(8,128)(2,1)} %copy-done.19, bf16[192,192]{1,0:T(8,128)(2,1)} %constant.25.clone.place_ref, bf16[2,256,2048]{2,1,0:T(8,128)(2,1)} %refs_0_.3, bf16[256,2048]{1,0:T(8,128)(2,1)} %copy-done.10, ...), custom_call_target="tpu_custom_call" | custom-call | tf_op jit(solution)/shard_map/pallas_call | solution.py:394
  163.7 11.6 %all-to-all-start.1 = ((bf16[64,24,512]{2,1,0:T(8,128)(2,1)}), bf16[64,24,512]{2,1,0:T(8,128)(2,1)}, u32[]{:S(2)}, u32[]{:S(2)}) async-start(bf16[64,24,512]{2,1,0:T(8,128)(2,1)} %bitcast.34), calls=%async_computation.1 | async-start | bytes 3145728 | tf_op jit(solution)/shard_map/all_to_all | solution.py:365
  178.1 2.5 collective-permute-start.13
  180.9 2.5 collective-permute-start.15
  183.4 43.2 %collective-permute-done.18.refs_2_ = bf16[176,2048]{1,0:T(8,128)(2,1)} collective-permute-done((bf16[176,2048]{1,0:T(8,128)(2,1)S(1)}, bf16[176,2048]{1,0:T(8,128)(2,1)}, u32[]{:S(2)}, u32[]{:S(2)}) %collective-permute-start.18) | collective-permute-done | bytes 720928 | tf_op jit(solution)/shard_map/ppermute | solution.py:328
  231.4 5.8 %shard_map.176 = bf16[384,512]{1,0:T(8,128)(2,1)} custom-call(bf16[1536,512]{1,0:T(8,128)(2,1)} %collective-permute-done.16.x_ref, bf16[192,192]{1,0:T(8,128)(2,1)} %constant.24.clone.place_ref, bf16[2,2048,256]{2,1,0:T(8,128)(2,1)} %ga.9, bf16[2,2048,256]{2,1,0:T(8,128)(2,1)} %ua.9, bf16[2048,256]{1,0:T(8,128)(2,1)} %copy-done.4, ...), custom_call_target="tpu_custom_call" | custom-call | tf_op jit(solution)/shard_map/pallas_call | solution.py:371
  238.8 5.7 %shard_map.175.mine_ref = bf16[384,512]{1,0:T(8,128)(2,1)} custom-call(bf16[1536,512]{1,0:T(8,128)(2,1)} %bitcast.15.x_ref, bf16[192,192]{1,0:T(8,128)(2,1)} %constant.24.clone.place_ref, bf16[2,2048,256]{2,1,0:T(8,128)(2,1)} %ga.9, bf16[2,2048,256]{2,1,0:T(8,128)(2,1)} %ua.9, bf16[2048,256]{1,0:T(8,128)(2,1)} %copy-done.4, bf16[1024,256]{1,0:T(8,128)(2,1)} %copy-done.7, ...), custom_call_target="tpu_custom_call" | custom-call | tf_op jit(solution)/shard_map/pallas_call | solution.py:371
  244.6 6.7 %collective-permute-done.21.refs_5_ = bf16[80,2048]{1,0:T(8,128)(2,1)S(1)} collective-permute-done((bf16[80,2048]{1,0:T(8,128)(2,1)S(1)}, bf16[80,2048]{1,0:T(8,128)(2,1)S(1)}, u32[]{:S(2)}, u32[]{:S(2)}) %collective-permute-start.21) | collective-permute-done | bytes 327712 | tf_op jit(solution)/shard_map/ppermute | solution.py:328
  253.1 6.6 %shard_map.177 = bf16[1536,512]{1,0:T(8,128)(2,1)} custom-call(bf16[384,512]{1,0:T(8,128)(2,1)} %shard_map.175.mine_ref, bf16[384,512]{1,0:T(8,128)(2,1)} %copy-done.18, bf16[192,192]{1,0:T(8,128)(2,1)} %constant.25.clone.place_ref, bf16[2,256,2048]{2,1,0:T(8,128)(2,1)} %refs_0_.3, bf16[2,256,2048]{2,1,0:T(8,128)(2,1)} %collective-permute-done.10.refs_2_.refs_1_, ...), custom_call_target="tpu_custom_call" | custom-call | tf_op jit(solution)/shard_map/pallas_call | solution.py:394
  259.8 12.4 %all-to-all-start.3 = ((bf16[64,24,512]{2,1,0:T(8,128)(2,1)}), bf16[64,24,512]{2,1,0:T(8,128)(2,1)S(1)}, u32[]{:S(2)}, u32[]{:S(2)}) async-start(bf16[64,24,512]{2,1,0:T(8,128)(2,1)} %bitcast.35), calls=%async_computation.3 | async-start | bytes 3145728 | tf_op jit(solution)/shard_map/all_to_all | solution.py:365
  272.2 2.6 collective-permute-start.1
  277.3 9.2 %collective-permute-done.1.other_ref = bf16[128,2048]{1,0:T(8,128)(2,1)S(1)} collective-permute-done((bf16[128,2048]{1,0:T(8,128)(2,1)S(1)}, bf16[128,2048]{1,0:T(8,128)(2,1)S(1)}, u32[]{:S(2)}, u32[]{:S(2)}) %collective-permute-start.1) | collective-permute-done | bytes 524320 | tf_op jit(solution)/shard_map/ppermute | solution.py:328
  287.5 11.2 %collective-permute-done.3.ub = bf16[2048,128]{1,0:T(8,128)(2,1)S(1)} collective-permute-done((bf16[2048,128]{1,0:T(8,128)(2,1)S(1)}, bf16[2048,128]{1,0:T(8,128)(2,1)S(1)}, u32[]{:S(2)}, u32[]{:S(2)}) %collective-permute-start.3) | collective-permute-done | bytes 524320 | tf_op jit(solution)/shard_map/ppermute | solution.py:328
  299.6 10.5 %collective-permute-done.4.db = bf16[128,2048]{1,0:T(8,128)(2,1)} collective-permute-done((bf16[128,2048]{1,0:T(8,128)(2,1)}, bf16[128,2048]{1,0:T(8,128)(2,1)}, u32[]{:S(2)}, u32[]{:S(2)}) %collective-permute-start.4) | collective-permute-done | bytes 524320 | tf_op jit(solution)/shard_map/ppermute | solution.py:328
  310.1 5.2 %shard_map.169 = (f32[128,2048]{1,0:T(8,128)}, bf16[128,2048]{1,0:T(8,128)(2,1)}) custom-call(bf16[128,2048]{1,0:T(8,128)(2,1)} %get-tuple-element.9.own_ref.h_ref, bf16[128,2048]{1,0:T(8,128)(2,1)} %copy-done.15, bf16[2048,128]{1,0:T(8,128)(2,1)} %ga.5, bf16[2048,128]{1,0:T(8,128)(2,1)} %ua.5, bf16[128,2048]{1,0:T(8,128)(2,1)} %da.1, ...), custom_call_target="tpu_custom_call" | custom-call | tf_op jit(solution)/shard_map/pallas_call | solution.py:410
  320.3 11.4 %collective-permute-done.halo_ref = bf16[16,2048]{1,0:T(8,128)(2,1)S(1)} collective-permute-done((bf16[16,2048]{1,0:T(8,128)(2,1)S(1)}, bf16[16,2048]{1,0:T(8,128)(2,1)S(1)}, u32[]{:S(2)}, u32[]{:S(2)}) %collective-permute-start) | collective-permute-done | bytes 65568 | tf_op jit(solution)/shard_map/ppermute | solution.py:279
  332.4 4.7 %shard_map.167 = bf16[256,2048]{1,0:T(8,128)(2,1)} custom-call(s32[1]{0:T(128)} %bitcast.at_ref, bf16[256,2048]{1,0:T(8,128)(2,1)} %x_ref.2, f32[1,2048]{1,0:T(1,128)} %bitcast.39, bf16[16,2048]{1,0:T(8,128)(2,1)} %copy-done.23, bf16[4,512,512]{2,1,0:T(8,128)(2,1)} %pool_ref.1, f32[1,2048]{1,0:T(1,128)} %bitcast.41), custom_call_target="tpu_custom_call" | custom-call | tf_op jit(solution)/shard_map/pallas_call | solution.py:290
  337.1 4.7 %shard_map.173 = (f32[128,2048]{1,0:T(8,128)}, bf16[256,384]{1,0:T(8,128)(2,1)}) custom-call(s32[1]{0:T(128)} %bitcast.3.at_ref, s32[512,4]{1,0:T(8,128)} %copy.18.ids_ref, f32[128,4]{1,0:T(8,128)} %copy.19.score_ref, f32[128,2048]{1,0:T(8,128)} %get-tuple-element.10.base_ref, bf16[1536,512]{1,0:T(8,128)(2,1)} %bitcast.13.r_ref, ...), custom_call_target="tpu_custom_call" | custom-call | tf_op jit(solution)/shard_map/pallas_call | solution.py:424
  343.2 4.1 %shard_map.178 = bf16[128,2048]{1,0:T(8,128)(2,1)} custom-call(f32[128,2048]{1,0:T(8,128)} %get-tuple-element.12.acc_ref, bf16[128,2048]{1,0:T(8,128)(2,1)} %copy-done.12, bf16[256,384]{1,0:T(8,128)(2,1)} %get-tuple-element.14.route_ref, bf16[1536,512]{1,0:T(8,128)(2,1)} %bitcast.33, bf16[192,192]{1,0:T(8,128)(2,1)} %constant.24.clone.place_ref), custom_call_target="tpu_custom_call" | custom-call | tf_op jit(solution)/shard_map/pallas_call | solution.py:432
  (96 shorter events, 35.7 us)
Async XLA Ops:
  4.6 52.3 %all-to-all-start = ((bf16[64,24,512]{2,1,0:T(8,128)(2,1)}), bf16[64,24,512]{2,1,0:T(8,128)(2,1)}, u32[]{:S(2)}, u32[]{:S(2)}) async-start(bf16[64,24,512]{2,1,0:T(8,128)(2,1)} %bitcast.36), calls=%async_computation | async-start | bytes 3145728 | tf_op jit(solution)/shard_map/all_to_all | solution.py:365
  17.9 53.3 %collective-permute-start.10 = (bf16[2,256,2048]{2,1,0:T(8,128)(2,1)}, bf16[2,256,2048]{2,1,0:T(8,128)(2,1)}, u32[]{:S(2)}, u32[]{:S(2)}) collective-permute-start(bf16[2,256,2048]{2,1,0:T(8,128)(2,1)} %refs_0_.3), channel_id=1, source_target_pairs={{1,2},{2,1},{3,0},{0,3},{5,6},{6,5},{7,4},{4,7},{9,10},{10,9},{11,... | collective-permute-start | bytes 6291464 | tf_op jit(solution)/shard_map/ppermute | solution.py:328
  24.3 39.1 %copy-start.2 = (bf16[2,2048,256]{2,1,0:T(8,128)(2,1)S(1)}, bf16[2,2048,256]{2,1,0:T(8,128)(2,1)}, u32[]{:S(2)}) copy-start(bf16[2,2048,256]{2,1,0:T(8,128)(2,1)} %ua.9) | copy-start | bytes 6291460
  56.9 106.7 %all-to-all-start.2 = ((bf16[64,24,512]{2,1,0:T(8,128)(2,1)}), bf16[64,24,512]{2,1,0:T(8,128)(2,1)}, u32[]{:S(2)}, u32[]{:S(2)}) async-start(bf16[64,24,512]{2,1,0:T(8,128)(2,1)} %bitcast.32), calls=%async_computation.2 | async-start | bytes 3145728 | tf_op jit(solution)/shard_map/all_to_all | solution.py:365
  64.6 24.3 %collective-permute-start.5 = (bf16[2048,256]{1,0:T(8,128)(2,1)S(1)}, bf16[2048,256]{1,0:T(8,128)(2,1)S(1)}, u32[]{:S(2)}, u32[]{:S(2)}) collective-permute-start(bf16[2048,256]{1,0:T(8,128)(2,1)S(1)} %get-tuple-element.19), channel_id=1, source_target_pairs={{0,1},{1,0},{2,3},{3,2},{4,5},{5,4},{6,7},{7,6},{8,9},{9,8},{10,11... | collective-permute-start | bytes 3145736 | tf_op jit(solution)/shard_map/ppermute | solution.py:328
  65.9 45.4 %collective-permute-start.6 = (bf16[2048,256]{1,0:T(8,128)(2,1)S(1)}, bf16[2048,256]{1,0:T(8,128)(2,1)S(1)}, u32[]{:S(2)}, u32[]{:S(2)}) collective-permute-start(bf16[2048,256]{1,0:T(8,128)(2,1)S(1)} %slice_bitcast_fusion.3), channel_id=1, source_target_pairs={{0,1},{1,0},{2,3},{3,2},{4,5},{5,4},{6,7},{7,6},{8,9},{9,8},{10,11... | collective-permute-start | bytes 3145736 | tf_op jit(solution)/shard_map/ppermute | solution.py:328
  66.8 44.5 %collective-permute-start.7 = (bf16[1536,512]{1,0:T(8,128)(2,1)}, bf16[1536,512]{1,0:T(8,128)(2,1)}, u32[]{:S(2)}, u32[]{:S(2)}) collective-permute-start(bf16[1536,512]{1,0:T(8,128)(2,1)} %bitcast.7.x_ref), channel_id=1, source_target_pairs={{1,2},{2,1},{3,0},{0,3},{5,6},{6,5},{7,4},{4,7},{9,10},{10,9},{11,... | collective-permute-start | bytes 4718600 | tf_op jit(solution)/shard_map/ppermute | solution.py:328
  71.0 62.7 %collective-permute-start.9 = (bf16[256,2048]{1,0:T(8,128)(2,1)}, bf16[256,2048]{1,0:T(8,128)(2,1)S(1)}, u32[]{:S(2)}, u32[]{:S(2)}) collective-permute-start(bf16[256,2048]{1,0:T(8,128)(2,1)} %slice_bitcast_fusion.2), channel_id=1, source_target_pairs={{0,1},{1,0},{2,3},{3,2},{4,5},{5,4},{6,7},{7,6},{8,9},{9,8},{10,11... | collective-permute-start | bytes 3145736 | tf_op jit(solution)/shard_map/ppermute | solution.py:328
  73.6 82.8 %collective-permute-start.11 = (bf16[256,2048]{1,0:T(8,128)(2,1)}, bf16[256,2048]{1,0:T(8,128)(2,1)}, u32[]{:S(2)}, u32[]{:S(2)}) collective-permute-start(bf16[256,2048]{1,0:T(8,128)(2,1)} %slice_bitcast_fusion), channel_id=1, source_target_pairs={{0,1},{1,0},{2,3},{3,2},{4,5},{5,4},{6,7},{7,6},{8,9},{9,8},{10,11... | collective-permute-start | bytes 3145736 | tf_op jit(solution)/shard_map/ppermute | solution.py:328
  88.9 22.4 %copy-start.5 = (bf16[2048,256]{1,0:T(8,128)(2,1)}, bf16[2048,256]{1,0:T(8,128)(2,1)S(1)}, u32[]{:S(2)}) copy-start(bf16[2048,256]{1,0:T(8,128)(2,1)S(1)} %collective-permute-done.5.ub) | copy-start | bytes 3145732
  118.0 38.3 %collective-permute-start.8 = (bf16[384,512]{1,0:T(8,128)(2,1)}, bf16[384,512]{1,0:T(8,128)(2,1)S(1)}, u32[]{:S(2)}, u32[]{:S(2)}) collective-permute-start(bf16[384,512]{1,0:T(8,128)(2,1)} %shard_map.171), channel_id=1, source_target_pairs={{1,2},{2,1},{3,0},{0,3},{5,6},{6,5},{7,4},{4,7},{9,10},{10,9},{11,... | collective-permute-start | bytes 1179656 | tf_op jit(solution)/shard_map/ppermute | solution.py:328
  133.7 22.6 %copy-start.10 = (bf16[256,2048]{1,0:T(8,128)(2,1)}, bf16[256,2048]{1,0:T(8,128)(2,1)S(1)}, u32[]{:S(2)}) copy-start(bf16[256,2048]{1,0:T(8,128)(2,1)S(1)} %collective-permute-done.9.refs_1_) | copy-start | bytes 3145732
  163.7 96.1 %all-to-all-start.1 = ((bf16[64,24,512]{2,1,0:T(8,128)(2,1)}), bf16[64,24,512]{2,1,0:T(8,128)(2,1)}, u32[]{:S(2)}, u32[]{:S(2)}) async-start(bf16[64,24,512]{2,1,0:T(8,128)(2,1)} %bitcast.34), calls=%async_computation.1 | async-start | bytes 3145728 | tf_op jit(solution)/shard_map/all_to_all | solution.py:365
  175.3 54.9 %collective-permute-start.16 = (bf16[1536,512]{1,0:T(8,128)(2,1)}, bf16[1536,512]{1,0:T(8,128)(2,1)}, u32[]{:S(2)}, u32[]{:S(2)}) collective-permute-start(bf16[1536,512]{1,0:T(8,128)(2,1)} %bitcast.15.x_ref), channel_id=1, source_target_pairs={{0,1},{1,0},{2,3},{3,2},{4,5},{5,4},{6,7},{7,6},{8,9},{9,8},{10,11... | collective-permute-start | bytes 4718600 | tf_op jit(solution)/shard_map/ppermute | solution.py:328
  177.7 48.8 %collective-permute-start.18 = (bf16[176,2048]{1,0:T(8,128)(2,1)S(1)}, bf16[176,2048]{1,0:T(8,128)(2,1)}, u32[]{:S(2)}, u32[]{:S(2)}) collective-permute-start(bf16[176,2048]{1,0:T(8,128)(2,1)S(1)} %slice_bitcast_fusion.5), channel_id=1, source_target_pairs={{0,1},{1,0},{2,3},{3,2},{4,5},{5,4},{6,7},{7,6},{8,9},{9,8},{10,11... | collective-permute-start | bytes 2162696 | tf_op jit(solution)/shard_map/ppermute | solution.py:328
  178.1 52.1 %collective-permute-start.13 = (bf16[2048,256]{1,0:T(8,128)(2,1)}, bf16[2048,256]{1,0:T(8,128)(2,1)S(1)}, u32[]{:S(2)}, u32[]{:S(2)}) collective-permute-start(bf16[2048,256]{1,0:T(8,128)(2,1)} %get-tuple-element.18), channel_id=1, source_target_pairs={{1,2},{2,1},{3,0},{0,3},{5,6},{6,5},{7,4},{4,7},{9,10},{10,9},{11,... | collective-permute-start | bytes 3145736 | tf_op jit(solution)/shard_map/ppermute | solution.py:328
  180.6 49.4 %collective-permute-start.14 = (bf16[1024,256]{1,0:T(8,128)(2,1)S(1)}, bf16[1024,256]{1,0:T(8,128)(2,1)S(1)}, u32[]{:S(2)}, u32[]{:S(2)}) collective-permute-start(bf16[1024,256]{1,0:T(8,128)(2,1)S(1)} %get-tuple-element.17), channel_id=1, source_target_pairs={{1,2},{2,1},{3,0},{0,3},{5,6},{6,5},{7,4},{4,7},{9,10},{10,9},{11,... | collective-permute-start | bytes 1572872 | tf_op jit(solution)/shard_map/ppermute | solution.py:328
  180.9 49.2 %collective-permute-start.15 = (bf16[1024,256]{1,0:T(8,128)(2,1)S(1)}, bf16[1024,256]{1,0:T(8,128)(2,1)S(1)}, u32[]{:S(2)}, u32[]{:S(2)}) collective-permute-start(bf16[1024,256]{1,0:T(8,128)(2,1)S(1)} %get-tuple-element.16), channel_id=1, source_target_pairs={{1,2},{2,1},{3,0},{0,3},{5,6},{6,5},{7,4},{4,7},{9,10},{10,9},{11,... | collective-permute-start | bytes 1572872 | tf_op jit(solution)/shard_map/ppermute | solution.py:328
  226.6 24.8 %collective-permute-start.20 = (bf16[176,2048]{1,0:T(8,128)(2,1)}, bf16[176,2048]{1,0:T(8,128)(2,1)S(1)}, u32[]{:S(2)}, u32[]{:S(2)}) collective-permute-start(bf16[176,2048]{1,0:T(8,128)(2,1)} %collective-permute-done.18.refs_2_), channel_id=1, source_target_pairs={{1,2},{2,1},{3,0},{0,3},{5,6},{6,5},{7,4},{4,7},{9,10},{10,9},{11,... | collective-permute-start | bytes 2162696 | tf_op jit(solution)/shard_map/ppermute | solution.py:328
  230.1 8.6 %collective-permute-start.19 = (bf16[80,2048]{1,0:T(8,128)(2,1)S(1)}, bf16[80,2048]{1,0:T(8,128)(2,1)S(1)}, u32[]{:S(2)}, u32[]{:S(2)}) collective-permute-start(bf16[80,2048]{1,0:T(8,128)(2,1)S(1)} %slice_bitcast_fusion.8), channel_id=1, source_target_pairs={{0,1},{1,0},{2,3},{3,2},{4,5},{5,4},{6,7},{7,6},{8,9},{9,8},{10,11... | collective-permute-start | bytes 983048 | tf_op jit(solution)/shard_map/ppermute | solution.py:328
  237.2 14.2 %collective-permute-start.17 = (bf16[384,512]{1,0:T(8,128)(2,1)}, bf16[384,512]{1,0:T(8,128)(2,1)S(1)}, u32[]{:S(2)}, u32[]{:S(2)}) collective-permute-start(bf16[384,512]{1,0:T(8,128)(2,1)} %shard_map.176), channel_id=1, source_target_pairs={{0,1},{1,0},{2,3},{3,2},{4,5},{5,4},{6,7},{7,6},{8,9},{9,8},{10,11... | collective-permute-start | bytes 1179656 | tf_op jit(solution)/shard_map/ppermute | solution.py:328
  238.6 12.7 %collective-permute-start.21 = (bf16[80,2048]{1,0:T(8,128)(2,1)S(1)}, bf16[80,2048]{1,0:T(8,128)(2,1)S(1)}, u32[]{:S(2)}, u32[]{:S(2)}) collective-permute-start(bf16[80,2048]{1,0:T(8,128)(2,1)S(1)} %collective-permute-done.19.refs_3_), channel_id=1, source_target_pairs={{1,2},{2,1},{3,0},{0,3},{5,6},{6,5},{7,4},{4,7},{9,10},{10,9},{11,... | collective-permute-start | bytes 983048 | tf_op jit(solution)/shard_map/ppermute | solution.py:328
  259.8 82.1 %all-to-all-start.3 = ((bf16[64,24,512]{2,1,0:T(8,128)(2,1)}), bf16[64,24,512]{2,1,0:T(8,128)(2,1)S(1)}, u32[]{:S(2)}, u32[]{:S(2)}) async-start(bf16[64,24,512]{2,1,0:T(8,128)(2,1)} %bitcast.35), calls=%async_computation.3 | async-start | bytes 3145728 | tf_op jit(solution)/shard_map/all_to_all | solution.py:365
  272.2 14.3 %collective-permute-start.1 = (bf16[128,2048]{1,0:T(8,128)(2,1)S(1)}, bf16[128,2048]{1,0:T(8,128)(2,1)S(1)}, u32[]{:S(2)}, u32[]{:S(2)}) collective-permute-start(bf16[128,2048]{1,0:T(8,128)(2,1)S(1)} %copy-done.9), channel_id=1, source_target_pairs={{1,2},{2,1},{3,0},{0,3},{5,6},{6,5},{7,4},{4,7},{9,10},{10,9},{11,... | collective-permute-start | bytes 1572872 | tf_op jit(solution)/shard_map/ppermute | solution.py:328
  274.8 12.7 %collective-permute-start.2 = (bf16[2048,128]{1,0:T(8,128)(2,1)S(1)}, bf16[2048,128]{1,0:T(8,128)(2,1)S(1)}, u32[]{:S(2)}, u32[]{:S(2)}) collective-permute-start(bf16[2048,128]{1,0:T(8,128)(2,1)S(1)} %copy-done.13), channel_id=1, source_target_pairs={{0,1},{1,0},{2,3},{3,2},{4,5},{5,4},{6,7},{7,6},{8,9},{9,8},{10,11... | collective-permute-start | bytes 1572872 | tf_op jit(solution)/shard_map/ppermute | solution.py:328
  274.8 24.0 %collective-permute-start.3 = (bf16[2048,128]{1,0:T(8,128)(2,1)S(1)}, bf16[2048,128]{1,0:T(8,128)(2,1)S(1)}, u32[]{:S(2)}, u32[]{:S(2)}) collective-permute-start(bf16[2048,128]{1,0:T(8,128)(2,1)S(1)} %copy-done.14), channel_id=1, source_target_pairs={{0,1},{1,0},{2,3},{3,2},{4,5},{5,4},{6,7},{7,6},{8,9},{9,8},{10,11... | collective-permute-start | bytes 1572872 | tf_op jit(solution)/shard_map/ppermute | solution.py:328
  276.3 33.9 %collective-permute-start.4 = (bf16[128,2048]{1,0:T(8,128)(2,1)}, bf16[128,2048]{1,0:T(8,128)(2,1)}, u32[]{:S(2)}, u32[]{:S(2)}) collective-permute-start(bf16[128,2048]{1,0:T(8,128)(2,1)} %da.1), channel_id=1, source_target_pairs={{0,1},{1,0},{2,3},{3,2},{4,5},{5,4},{6,7},{7,6},{8,9},{9,8},{10,11... | collective-permute-start | bytes 1572872 | tf_op jit(solution)/shard_map/ppermute | solution.py:328
  277.3 38.2 %copy-start.24 = (f32[2048]{0:T(1024)S(1)}, f32[2048]{0:T(1024)}, u32[]{:S(2)}) copy-start(f32[2048]{0:T(1024)} %param.17) | copy-start | bytes 24580
  277.3 41.4 %copy-start.22 = (s32[512,4]{0,1:T(4,128)S(1)}, s32[512,4]{0,1:T(4,128)}, u32[]{:S(2)}) copy-start(s32[512,4]{0,1:T(4,128)} %param.22) | copy-start | bytes 24580
  277.3 42.2 %copy-start.25 = (f32[128,4]{0,1:T(4,128)S(1)}, f32[128,4]{0,1:T(4,128)}, u32[]{:S(2)}) copy-start(f32[128,4]{0,1:T(4,128)} %param.23) | copy-start | bytes 6148
  315.3 26.6 %collective-permute-start.12 = (bf16[128,2048]{1,0:T(8,128)(2,1)}, bf16[128,2048]{1,0:T(8,128)(2,1)S(1)}, u32[]{:S(2)}, u32[]{:S(2)}) collective-permute-start(bf16[128,2048]{1,0:T(8,128)(2,1)} %get-tuple-element.13), channel_id=1, source_target_pairs={{1,2},{2,1},{3,0},{0,3},{5,6},{6,5},{7,4},{4,7},{9,10},{10,9},{11,... | collective-permute-start | bytes 1572872 | tf_op jit(solution)/shard_map/ppermute | solution.py:328
  316.4 15.3 %collective-permute-start = (bf16[16,2048]{1,0:T(8,128)(2,1)S(1)}, bf16[16,2048]{1,0:T(8,128)(2,1)S(1)}, u32[]{:S(2)}, u32[]{:S(2)}) collective-permute-start(bf16[16,2048]{1,0:T(8,128)(2,1)S(1)} %fusion.2), channel_id=1, source_target_pairs={{0,1},{1,2},{2,3},{3,4},{4,5},{5,6},{6,7},{7,8},{8,9},{9,10},{10,1... | collective-permute-start | bytes 196616 | tf_op jit(solution)/shard_map/ppermute | solution.py:279
  (20 other events, 101.9 us)
